TPU v7x, 128 devices: a whole 4x4x4 slice. The times are simulated.
128 devices in a mesh: sp: 16 (over z, y), dp: 8 (over x, core).
Axes of the slice: x: 4, y: 4, z: 4, core: 2. Of those that a mesh axis runs over, the one named last changes fastest.
Arguments:
- residual: bfloat16 [8, 2048, 2048], P('dp', 'sp'), may hold values from -6 to 6
- query: bfloat16 [8, 2048, 1536], P('dp', 'sp'), may hold values from -64 to 64
- latent: bfloat16 [8, 2048, 256], P('dp', 'sp'), may hold values from -6 to 6
- rope_key: bfloat16 [8, 2048, 32], P('dp', 'sp'), may hold values from -64 to 64
- latent_gain: float32 [256], replicated, may hold values from 0.1 to 1.9
- query_gain: float32 [96], replicated, may hold values from 0.7 to 5.6
- key_gain: float32 [96], replicated, may hold values from 0.7 to 5.6
- key_weight: bfloat16 [256, 1024], replicated, may hold values from -0.375 to 0.375
- value_weight: bfloat16 [256, 1024], replicated, may hold values from -0.375 to 0.375
- mix_gain: float32 [1024], replicated, may hold values from 0.1 to 1.9
- out_weight: bfloat16 [1024, 2048], replicated, may hold values from -0.1875 to 0.1875
- ffn_gain: float32 [2048], replicated, may hold values from 0.1 to 1.9
- expert_choice: int32 [8, 2048, 2], P('dp', 'sp'), may hold values from 0 to 127, as said below
- group_prob: float32 [8, 2048], P('dp', 'sp'), may hold values from 0.25 to 1
- expert_prob: float32 [8, 2048, 2], P('dp', 'sp'), may hold values from 0.05 to 1
- gate_weight: bfloat16 [128, 2048, 512], P(('sp', 'dp')), may hold values from -0.125 to 0.125
- up_weight: bfloat16 [128, 2048, 512], P(('sp', 'dp')), may hold values from -0.125 to 0.125
- down_weight: bfloat16 [128, 512, 2048], P(('sp', 'dp')), may hold values from -0.25 to 0.25
Outputs:
- layer_out: bfloat16 [8, 2048, 2048], P('dp', 'sp')
Inputs may be any that keep to these rules, and one draw needn't show every extreme that they name: `expert_choice`: A token's two experts differ and lie in one group of 32 consecutive expert numbers. In each aligned block of 128 tokens (the tokens of one device) no expert is named more than 4 times, and every expert of one group is named exactly 4 times in every block.
All inputs are finite; a program needn't handle non-finite values.
Results may differ from a plain program's by a relative error of at most 0.012.
The roundings to bfloat16 on the way count: a program that leaves them out, or rounds other values in their place, can miss the bound.
Values may be sent and summed in bfloat16 or wider, within the bound.
A program may use at most 64 MiB of HBM per device.

v0:
```python
import functools

import jax
import jax.numpy as jnp
from jax import lax
from jax.experimental import pallas as pl
from jax.experimental.pallas import tpu as pltpu
from jax.sharding import PartitionSpec as P

GROUPS = 4
SPAN = 64


eps = 1e-06


def angles(offset, span_count, rope_width):
    position = (offset + jnp.arange(span_count, dtype=jnp.int32)).astype(jnp.float32)
    frequency = 10000.0 ** (-2.0 * jnp.arange(rope_width // 2, dtype=jnp.float32) / rope_width)
    return position[:, None] * frequency[None, :]


def dot32(a, b):
    return jnp.dot(a, b, preferred_element_type=jnp.float32)


def dot_t(a, b):
    return lax.dot_general(a, b, (((0,), (0,)), ((), ())), preferred_element_type=jnp.float32)


def expert_kernel(
    n_y,
    n_dp,
    cap,
    rows,
    normed_ref,
    info_ref,
    pick_ref,
    stream_ref,
    gate_hbm,
    up_hbm,
    down_hbm,
    out_ref,
    gate_ref,
    up_ref,
    down_ref,
    out1,
    in1,
    out2,
    arrive,
    served,
    back2,
    merged,
    home,
    acc,
    w_sem,
    s1,
    r1,
    s2,
    r2,
    s3,
    r3,
    s4,
    r4,
    l_sem,
):
    peers = n_y * n_dp
    width = normed_ref.shape[1]
    sp = lax.axis_index("sp")
    dp = lax.axis_index("dp")
    plane = sp // n_y
    row = sp % n_y
    mine = row * n_dp + dp

    def column(k):
        return {"sp": ((plane + k) % GROUPS) * n_y + row, "dp": dp}

    def peer(j):
        other = (mine + j) % peers
        return {"sp": plane * n_y + other // n_dp, "dp": other % n_dp}

    loads = [
        pltpu.make_async_copy(gate_hbm, gate_ref, w_sem.at[0]),
        pltpu.make_async_copy(up_hbm, up_ref, w_sem.at[1]),
        pltpu.make_async_copy(down_hbm, down_ref, w_sem.at[2]),
    ]
    for load in loads:
        load.start()
    barrier = pltpu.get_barrier_semaphore()
    for k in range(1, GROUPS):
        pl.semaphore_signal(barrier, inc=1, device_id=column(k), device_id_type=pl.DeviceIdType.MESH)
    for j in range(1, peers):
        pl.semaphore_signal(barrier, inc=1, device_id=peer(j), device_id_type=pl.DeviceIdType.MESH)

    def remote(src, dst, send, recv, target):
        return pltpu.make_async_remote_copy(
            src_ref=src,
            dst_ref=dst,
            send_sem=send,
            recv_sem=recv,
            device_id=target,
            device_id_type=pl.DeviceIdType.MESH,
        )

    first = {}

    def pack(k, target):
        picks = pick_ref[(plane + k) % GROUPS]
        target[k, :, :width] = dot32(picks, normed_ref[...]).astype(jnp.bfloat16)
        target[k, :, width:] = dot32(picks, info_ref[...]).astype(jnp.bfloat16)

    for k in (2, 1, 3):
        pack(k, out1)
        if k == 2:
            pl.semaphore_wait(barrier, GROUPS - 1 + peers - 1)
        first[k] = remote(out1.at[k], in1.at[k], s1.at[k], r1.at[k], column(k))
        first[k].start()
    pack(0, in1)

    def slots(k):
        info = in1[k, :, width:].astype(jnp.float32)
        place = lax.broadcasted_iota(jnp.int32, (rows, peers * cap), 1).astype(jnp.float32)
        return place == info[:, 0:1], place == info[:, 1:2], info

    second = {}

    def scatter(k):
        if k:
            first[k].wait_recv()
        at0, at1, _ = slots(k)
        choose = (at0.astype(jnp.float32) + at1.astype(jnp.float32)).astype(jnp.bfloat16)
        placed = dot_t(choose, in1[k, :, :width]).astype(jnp.bfloat16)
        for e in range(peers):
            out2[k, e] = placed[e * cap : (e + 1) * cap]
        second[k] = [
            remote(
                out2.at[k, (mine + j) % peers], arrive.at[k, j], s2.at[k, j], r2.at[k, j], peer(j)
            )
            for j in range(1, peers)
        ]
        for copy in second[k]:
            copy.start()
        arrive[k, 0] = out2[k, mine]

    third = {}

    def serve(k):
        for copy in second[k]:
            copy.wait_recv()
        if k == 2:
            for load in loads:
                load.wait()
        given = arrive[k].reshape(peers * cap, width)
        gate_act = dot32(given, gate_ref[...])
        upward = dot32(given, up_ref[...])
        hidden = (gate_act * (1.0 / (1.0 + jnp.exp(-gate_act))) * upward).astype(jnp.bfloat16)
        result = dot32(hidden, down_ref[...]).astype(jnp.bfloat16)
        for j in range(peers):
            served[k, j] = result[j * cap : (j + 1) * cap]
        third[k] = [
            remote(
                served.at[k, j], back2.at[k, mine], s3.at[k, j], r3.at[k, peers - j], peer(peers - j)
            )
            for j in range(1, peers)
        ]
        for copy in third[k]:
            copy.start()
        back2[k, mine] = served[k, 0]

    fourth = {}

    def merge(k):
        for copy in third[k]:
            copy.wait_recv()
        at0, at1, info = slots(k)
        high = jnp.where(at0, info[:, 2:3], 0.0) + jnp.where(at1, info[:, 4:5], 0.0)
        low = jnp.where(at0, info[:, 3:4], 0.0) + jnp.where(at1, info[:, 5:6], 0.0)
        got = back2[k].reshape(peers * cap, width)
        total = dot32(high.astype(jnp.bfloat16), got) + dot32(low.astype(jnp.bfloat16), got)
        if k:
            merged[k] = total.astype(jnp.bfloat16)
            fourth[k] = remote(merged.at[k], home.at[k], s4.at[k], r4.at[k], column(GROUPS - k))
            fourth[k].start()
        else:
            acc[...] = stream_ref[...] + dot_t(pick_ref[plane], total.astype(jnp.bfloat16))

    scatter(0)
    scatter(2)
    scatter(1)
    scatter(3)
    serve(2)
    serve(1)
    serve(3)
    merge(2)
    merge(1)
    merge(3)
    serve(0)
    merge(0)
    for k in (2, 1, 3):
        fourth[k].wait_recv()
        acc[...] += dot_t(pick_ref[(plane + k) % GROUPS], home[k])
    out_ref[...] = acc[...].astype(jnp.bfloat16)
    for k in range(GROUPS):
        if k:
            first[k].wait_send()
            fourth[k].wait_send()
        for copy in second[k] + third[k]:
            copy.wait_send()


def attention_kernel(
    n_sp,
    n_y,
    heads,
    nope,
    rope,
    value_width,
    query_ref,
    packed_ref,
    latent_gain_ref,
    query_gain_ref,
    query_swap_ref,
    key_gain_ref,
    key_swap_ref,
    cos_ref,
    sin_ref,
    key_weight_ref,
    value_weight_ref,
    residual_ref,
    mix_gain_ref,
    ffn_gain_ref,
    out_weight_hbm,
    stream_ref,
    normed_ref,
    out_weight_ref,
    queries_in,
    packed_in,
    queries,
    keys,
    values,
    heads_out,
    token_in,
    mixed,
    w_sem,
    sq,
    rq,
    sz,
    rz,
    sy,
    ry,
    so,
    ro,
):
    bf = jnp.bfloat16
    tok = residual_ref.shape[0]
    length = n_sp * tok
    qk = nope + rope
    lat = packed_ref.shape[1]
    me = lax.axis_index("sp")
    plane = me // n_y
    row = me % n_y
    load = pltpu.make_async_copy(out_weight_hbm, out_weight_ref, w_sem.at[0])
    load.start()

    def remote(src, dst, send, recv, target):
        return pltpu.make_async_remote_copy(
            src_ref=src,
            dst_ref=dst,
            send_sem=send,
            recv_sem=recv,
            device_id={"sp": target},
            device_id_type=pl.DeviceIdType.MESH,
        )

    barrier = pltpu.get_barrier_semaphore()
    for j in range(1, n_sp):
        pl.semaphore_signal(
            barrier,
            inc=1,
            device_id={"sp": (me + j) % n_sp},
            device_id_type=pl.DeviceIdType.MESH,
        )
    pl.semaphore_wait(barrier, n_sp - 1)

    down = []
    for k in range(1, GROUPS):
        target = ((plane + k) % GROUPS) * n_y + row
        down.append(remote(packed_ref, packed_in.at[me], sz.at[k], rz.at[k], target))
        down[-1].start()
    across = []

    def spread(k, source):
        index = ((plane + GROUPS - k) % GROUPS) * n_y + row
        for m in range(1, n_y):
            target = plane * n_y + (row + m) % n_y
            across.append(remote(source, packed_in.at[index], sy.at[k, m], ry.at[k, m], target))
            across[-1].start()

    spread(0, packed_ref)
    sent = []
    for j in range(1, n_sp):
        target = (me + j) % n_sp
        sent.append(remote(query_ref.at[target], queries_in.at[me], sq.at[j], rq.at[j], target))
        sent[-1].start()
    packed_in[me] = packed_ref[...]
    queries_in[me] = query_ref[me]
    for k in range(1, GROUPS):
        down[k - 1].wait_recv()
        spread(k, packed_in.at[((plane + GROUPS - k) % GROUPS) * n_y + row])
    for copy in across:
        copy.wait_recv()

    def selector(rows, columns, source):
        i = lax.broadcasted_iota(jnp.int32, (rows, columns), 0)
        c = lax.broadcasted_iota(jnp.int32, (rows, columns), 1)
        return (i == source(c)).astype(jnp.float32).astype(bf)

    half = rope // 2

    def swapped(c):
        return jnp.where(c < nope, -1, jnp.where(c < nope + half, c + half, c - half))

    def shape_head(plain, turned, gain, swap_gain, rows):
        scale = lax.rsqrt(jnp.sum(plain * plain, axis=-1, keepdims=True) / qk + eps)
        return (
            plain * scale * gain * cos_ref[rows, :] + turned * scale * swap_gain * sin_ref[rows, :]
        ).astype(bf)

    strips = lat // rope
    strip_rows = tok // strips

    def prepare(s, carry):
        rows = pl.ds(pl.multiple_of(s * tok, tok), tok)
        block = packed_in[s]
        raw = block[:tok].astype(jnp.float32)
        scale = lax.rsqrt(jnp.mean(raw * raw, axis=-1, keepdims=True) + eps)
        latent = (raw * scale * latent_gain_ref[...]).astype(bf)
        values[rows, :] = dot32(latent, value_weight_ref[...]).astype(bf)
        part = dot32(latent, key_weight_ref[...]).astype(bf)
        tail = block[tok:]
        plain_rope = jnp.concatenate(
            [
                dot32(tail, selector(lat, qk, lambda c: jnp.where(c < nope, -1, c - nope + i * rope)))
                for i in range(strips)
            ],
            axis=0,
        )
        turned = jnp.concatenate(
            [
                dot32(
                    tail,
                    selector(
                        lat, qk, lambda c: jnp.where(c < nope, -1, swapped(c) - nope + i * rope)
                    ),
                )
                for i in range(strips)
            ],
            axis=0,
        )
        for h in range(heads):
            plain = plain_rope + dot32(
                part, selector(heads * nope, qk, lambda c: jnp.where(c < nope, c + h * nope, -1))
            )
            keys[h, rows, :] = shape_head(
                plain, turned, key_gain_ref[...], key_swap_ref[...], rows
            )
        return carry

    lax.fori_loop(0, n_sp, prepare, 0)
    for copy in sent:
        copy.wait_recv()

    def prepare_queries(s, carry):
        rows = pl.ds(pl.multiple_of(s * tok, tok), tok)
        raw = queries_in[s]
        for h in range(heads):
            plain = dot32(raw, selector(heads * qk, qk, lambda c: c + h * qk))
            turned = dot32(
                raw,
                selector(
                    heads * qk, qk, lambda c: jnp.where(c < nope, -1, swapped(c) + h * qk)
                ),
            )
            queries[h, rows, :] = shape_head(
                plain, turned, query_gain_ref[...], query_swap_ref[...], rows
            )
        return carry

    lax.fori_loop(0, n_sp, prepare_queries, 0)

    blocks = 4
    block_rows = length // blocks
    for b in range(blocks):
        first_row = b * block_rows
        last_row = first_row + block_rows
        total = None
        lane = lax.broadcasted_iota(jnp.int32, (block_rows, heads * value_width), 1)
        q_pos = first_row + lax.broadcasted_iota(jnp.int32, (block_rows, last_row), 0)
        k_pos = lax.broadcasted_iota(jnp.int32, (block_rows, last_row), 1)
        allowed = k_pos // SPAN <= q_pos // SPAN
        for h in range(heads):
            scores = lax.dot_general(
                queries[h, first_row:last_row],
                keys[h, :last_row],
                (((1,), (1,)), ((), ())),
                preferred_element_type=jnp.float32,
            ) * (qk ** (-0.5))
            scores = jnp.where(allowed, scores, -1e30)
            raised = jnp.exp(scores - jnp.max(scores, axis=-1, keepdims=True))
            row_sum = jnp.sum(raised, axis=-1, keepdims=True)
            mine = dot32(raised.astype(bf), values[:last_row]) / row_sum
            total = mine if total is None else jnp.where(lane < h * value_width, total, mine)
        total = total.astype(bf)
        for t in range(block_rows // tok):
            index = first_row // tok + t
            heads_out[index] = total[t * tok : (t + 1) * tok]

            @pl.when(index != me)
            def _():
                remote(
                    heads_out.at[index], token_in.at[me], so.at[index], ro.at[me], index
                ).start()

    token_in[me] = heads_out[me]
    load.wait()
    for j in range(1, n_sp):
        other = (me + j) % n_sp
        remote(
            heads_out.at[other], token_in.at[other], so.at[other], ro.at[other], other
        ).wait()
    wide = heads * value_width
    square = None
    for s in range(n_sp):
        piece = token_in[s].astype(jnp.float32)
        part = jnp.sum(piece * piece, axis=-1, keepdims=True)
        square = part if square is None else square + part
    scale = lax.rsqrt(square / (n_sp * wide) + eps)
    for s in range(n_sp):
        span = slice(s * wide, (s + 1) * wide)
        mixed[:, span] = (token_in[s].astype(jnp.float32) * scale * mix_gain_ref[:, span]).astype(bf)
    stream = residual_ref[...].astype(jnp.float32) + dot32(mixed[...], out_weight_ref[...])
    stream_ref[...] = stream
    scale = lax.rsqrt(jnp.mean(stream * stream, axis=-1, keepdims=True) + eps)
    normed_ref[...] = (stream * scale * ffn_gain_ref[...]).astype(bf)
    for copy in down + across + sent:
        copy.wait_send()


def attended(
    residual,
    query,
    latent,
    rope_key,
    latent_gain,
    query_gain,
    key_gain,
    key_weight,
    value_weight,
    mix_gain,
    out_weight,
    ffn_gain,
    head_count,
    nope,
    value_width,
):
    n_sp = lax.axis_size("sp")
    n_y = n_sp // GROUPS
    me = lax.axis_index("sp")
    tok, width = residual.shape
    rope = rope_key.shape[1]
    qk = nope + rope
    lat = latent.shape[1]
    heads = head_count // n_sp
    length = n_sp * tok
    half = rope // 2
    bf = jnp.bfloat16
    query_blocks = query.reshape(tok, n_sp, heads * qk).transpose(1, 0, 2)
    strips = lat // rope
    tail = rope_key.reshape(strips, tok // strips, rope).transpose(1, 0, 2).reshape(-1, lat)
    packed = jnp.concatenate([latent, tail], axis=0)
    phases = angles(0, length, rope)
    cos, sin = jnp.cos(phases), jnp.sin(phases)
    cos = jnp.concatenate([jnp.ones((length, nope), jnp.float32), cos, cos], axis=1)
    sin = jnp.concatenate([jnp.zeros((length, nope), jnp.float32), -sin, sin], axis=1)

    def swap(gain):
        return jnp.concatenate([gain[:nope], gain[nope + half :], gain[nope : nope + half]])

    key_own = lax.dynamic_slice_in_dim(key_weight, me * heads * nope, heads * nope, 1)
    value_own = lax.dynamic_slice_in_dim(value_weight, me * heads * value_width, heads * value_width, 1)
    vmem = pl.BlockSpec(memory_space=pltpu.VMEM)
    dma = pltpu.SemaphoreType.DMA
    wide = heads * value_width
    return pl.pallas_call(
        functools.partial(attention_kernel, n_sp, n_y, heads, nope, rope, value_width),
        out_shape=(
            jax.ShapeDtypeStruct((tok, width), jnp.float32),
            jax.ShapeDtypeStruct((tok, width), bf),
        ),
        in_specs=[vmem] * 14 + [pl.BlockSpec(memory_space=pl.ANY)],
        out_specs=(vmem, vmem),
        scratch_shapes=[
            pltpu.VMEM(out_weight.shape, bf),
            pltpu.VMEM((n_sp, tok, heads * qk), bf),
            pltpu.VMEM((n_sp,) + packed.shape, bf),
            pltpu.VMEM((heads, length, qk), bf),
            pltpu.VMEM((heads, length, qk), bf),
            pltpu.VMEM((length, wide), bf),
            pltpu.VMEM((n_sp, tok, wide), bf),
            pltpu.VMEM((n_sp, tok, wide), bf),
            pltpu.VMEM((tok, n_sp * wide), bf),
            dma((1,)),
            dma((n_sp,)),
            dma((n_sp,)),
            dma((GROUPS,)),
            dma((GROUPS,)),
            dma((GROUPS, n_y)),
            dma((GROUPS, n_y)),
            dma((n_sp,)),
            dma((n_sp,)),
        ],
        compiler_params=pltpu.CompilerParams(
            collective_id=1, has_side_effects=True, vmem_limit_bytes=48 * 1024 * 1024
        ),
    )(
        query_blocks,
        packed,
        latent_gain[None],
        query_gain[None],
        swap(query_gain)[None],
        key_gain[None],
        swap(key_gain)[None],
        cos,
        sin,
        key_own,
        value_own,
        residual,
        mix_gain[None],
        ffn_gain[None],
        out_weight,
    )


def routed(normed, stream, choice, group_prob, share, gate, up, down, expert_total):
    tok_rows, width = normed.shape
    n_y = lax.axis_size("sp") // GROUPS
    n_dp = lax.axis_size("dp")
    per_group = expert_total // GROUPS
    cap = tok_rows * GROUPS // expert_total
    rows = per_group * cap // choice.shape[1]
    group = choice[:, 0] // per_group
    order = jnp.arange(tok_rows, dtype=jnp.int32)
    before = order[None, :] < order[:, None]
    rank = jnp.sum((before & (group[None, :] == group[:, None])).astype(jnp.int32), axis=1)
    line = group * rows + rank
    pick = (
        (line[None, :] == jnp.arange(GROUPS * rows, dtype=jnp.int32)[:, None])
        .astype(jnp.bfloat16)
        .reshape(GROUPS, rows, tok_rows)
    )
    route = group_prob[:, None] * share / jnp.sum(share, axis=-1, keepdims=True)
    earlier = jnp.sum(
        (
            before[:, None, :, None] & (choice[:, :, None, None] == choice[None, None, :, :])
        ).astype(jnp.int32),
        axis=(2, 3),
    )
    position = (choice - group[:, None] * per_group) * cap + earlier
    high = lax.reduce_precision(route, 8, 7)
    low = route - high
    columns = jnp.concatenate(
        [
            position.astype(jnp.float32),
            jnp.stack([high[:, 0], low[:, 0], high[:, 1], low[:, 1]], axis=1),
            jnp.zeros((tok_rows, 122), jnp.float32),
        ],
        axis=1,
    ).astype(jnp.bfloat16)
    hidden = gate.shape[1]
    bf = jnp.bfloat16
    vmem = pl.BlockSpec(memory_space=pltpu.VMEM)
    hbm = pl.BlockSpec(memory_space=pl.ANY)
    dma = pltpu.SemaphoreType.DMA
    return pl.pallas_call(
        functools.partial(expert_kernel, n_y, n_dp, cap, rows),
        out_shape=jax.ShapeDtypeStruct((tok_rows, width), bf),
        in_specs=[vmem] * 4 + [hbm] * 3,
        out_specs=vmem,
        scratch_shapes=[
            pltpu.VMEM((width, hidden), bf),
            pltpu.VMEM((width, hidden), bf),
            pltpu.VMEM((hidden, width), bf),
            pltpu.VMEM((GROUPS, rows, width + 128), bf),
            pltpu.VMEM((GROUPS, rows, width + 128), bf),
            pltpu.VMEM((GROUPS, per_group, cap, width), bf),
            pltpu.VMEM((GROUPS, per_group, cap, width), bf),
            pltpu.VMEM((GROUPS, per_group, cap, width), bf),
            pltpu.VMEM((GROUPS, per_group, cap, width), bf),
            pltpu.VMEM((GROUPS, rows, width), bf),
            pltpu.VMEM((GROUPS, rows, width), bf),
            pltpu.VMEM((tok_rows, width), jnp.float32),
            dma((3,)),
            dma((GROUPS,)),
            dma((GROUPS,)),
            dma((GROUPS, per_group)),
            dma((GROUPS, per_group)),
            dma((GROUPS, per_group)),
            dma((GROUPS, per_group)),
            dma((GROUPS,)),
            dma((GROUPS,)),
            dma((1,)),
        ],
        compiler_params=pltpu.CompilerParams(
            collective_id=0, has_side_effects=True, vmem_limit_bytes=60 * 1024 * 1024
        ),
    )(normed, columns, pick, stream, gate, up, down)


def per_device(
    residual,
    query,
    latent,
    rope_key,
    latent_gain,
    query_gain,
    key_gain,
    key_weight,
    value_weight,
    mix_gain,
    out_weight,
    ffn_gain,
    expert_choice,
    group_prob,
    expert_prob,
    gate_weight,
    up_weight,
    down_weight,
):
    rope_width = rope_key.shape[2]
    qk_width = query_gain.shape[0]
    nope_width = qk_width - rope_width
    head_count = query.shape[2] // qk_width
    value_width = value_weight.shape[1] // head_count
    seq_devices = lax.axis_size("sp")
    stream, normed = attended(
        residual[0],
        query[0],
        latent[0],
        rope_key[0],
        latent_gain,
        query_gain,
        key_gain,
        key_weight,
        value_weight,
        mix_gain,
        out_weight,
        ffn_gain,
        head_count,
        nope_width,
        value_width,
    )
    expert_total = seq_devices * lax.axis_size("dp")
    return routed(
        normed,
        stream,
        expert_choice[0],
        group_prob[0],
        expert_prob[0],
        gate_weight[0],
        up_weight[0],
        down_weight[0],
        expert_total,
    )[None]


def solution(mesh):
    return jax.shard_map(
        per_device,
        mesh=mesh,
        in_specs=(
            P("dp", "sp", None),
            P("dp", "sp", None),
            P("dp", "sp", None),
            P("dp", "sp", None),
            P(),
            P(),
            P(),
            P(),
            P(),
            P(),
            P(),
            P(),
            P("dp", "sp", None),
            P("dp", "sp"),
            P("dp", "sp", None),
            P(("sp", "dp"), None, None),
            P(("sp", "dp"), None, None),
            P(("sp", "dp"), None, None),
        ),
        out_specs=P("dp", "sp", None),
        check_vma=False,
    )
```

profile of v0, /device:TPU:0, one launch (start us, length us, event | category | flops | bytes accessed | tf_op | source)
XLA Modules:
  0.0 138.9 jit_solution(10208252607109571599)
XLA Ops:
  0.0 3.7 %fusion = (f32[2048,16]{1,0:T(8,128)S(1)}, f32[2048,16]{1,0:T(8,128)S(1)}, f32[2048,16]{1,0:T(8,128)S(1)}) fusion(f32[16]{0:T(128)S(1)} %multiply_power_fusion, f32[2048]{0:T(1024)S(1)} %iota_convert_fusion), kind=kLoop, calls=%fused_computation.4 | loop fusion | flops 65536 | bytes 401472 | tf_op jit(solution)/shard_map/neg | solution.py:484
  3.8 0.0 copy-start.4
  3.8 0.0 copy-start.3
  3.8 0.0 copy-start.8
  3.8 0.0 copy-start.10
  3.8 1.1 pad_maximum_fusion
  5.0 0.0 copy-start.9
  5.0 0.0 copy-start.1
  5.0 0.0 copy-start.5
  5.0 0.0 copy-start.6
  5.0 0.0 copy-start.7
  5.1 1.0 constant_dynamic-slice_fusion
  6.1 0.0 copy-done.4
  6.1 0.1 fusion.8
  6.2 0.0 copy-done.3
  6.2 0.1 fusion.9
  6.3 0.1 maximum_bitcast_fusion
  6.3 0.0 copy-done.8
  6.3 0.9 copy.38
  7.3 1.3 copy.39
  8.5 0.0 copy-done.10
  8.5 0.1 copy.40
  8.7 0.1 reshape.85
  8.8 0.0 copy-done.9
  8.8 0.0 copy-done.1
  8.8 0.0 copy-done.5
  8.8 0.0 copy-done.6
  8.8 0.0 copy-done.7
  8.8 0.0 copy-start.12
  8.9 0.0 copy-start.11
  8.9 0.0 copy-start.13
  8.9 53.3 %shard_map.172 = (f32[128,2048]{1,0:T(8,128)S(1)}, bf16[128,2048]{1,0:T(8,128)(2,1)S(1)}) custom-call(bf16[16,128,96]{2,1,0:T(8,128)(2,1)S(1)} %bitcast.33, bf16[144,256]{1,0:T(8,128)(2,1)S(1)} %pad_maximum_fusion.2.packed_ref, f32[1,256]{1,0:T(1,128)S(1)} %bitcast.41, f32[1,96]{1,0:T(1,128)S(1)} %bitcast.36, f32[1,96]{1,0:T(1,128)S(1)} %get-tuple-element.29.query_swap_ref, ...), custom_call_target="tpu_custom_call" | custom-call | tf_op jit(solution)/shard_map/pallas_call | solution.py:494
  62.2 0.0 copy-start
  62.2 1.0 copy-done
  63.1 0.0 copy-start.2
  63.1 0.8 copy-done.2
  63.9 0.0 copy-done.12
  63.9 0.1 copy.43
  64.1 0.2 fusion.5
  64.2 0.1 subtract_multiply_fusion
  64.3 0.1 copy.47
  64.4 0.1 copy.45
  64.5 0.2 convert_reduce_fusion
  64.7 0.1 copy.49
  64.8 0.0 copy-done.11
  64.8 0.1 copy.48
  65.0 0.0 copy-done.13
  65.0 0.1 fusion.1
  65.1 0.1 fusion.6
  65.2 0.7 concatenate.24.info_ref
  65.9 0.2 convert_reduce_fusion.1
  66.2 0.7 compare_convert_fusion.pick_ref
  66.9 70.2 %shard_map.173 = bf16[128,2048]{1,0:T(8,128)(2,1)} custom-call(bf16[128,2048]{1,0:T(8,128)(2,1)} %copy-done.2, bf16[128,128]{1,0:T(8,128)(2,1)} %concatenate.24.info_ref, bf16[4,64,128]{2,1,0:T(8,128)(2,1)} %compare_convert_fusion.pick_ref, f32[128,2048]{1,0:T(8,128)} %copy-done, bf16[2048,512]{1,0:T(8,128)(2,1)} %bitcast.43, bf16[2048,512]{1,0:T(8,128)(2,1)} %bitcast.44, ...), custom_call_target="tpu_custom_call" | custom-call | tf_op jit(solution)/shard_map/pallas_call | solution.py:584
  137.0 1.9 %copy.51 = bf16[1,128,2048]{2,1,0:T(8,128)(2,1)} copy(bf16[1,128,2048]{2,1,0:T(8,128)(2,1)} %bitcast.42) | data formatting | bytes 1048576
  (15 shorter events, 0.1 us)
Async XLA Ops:
  3.8 2.3 %copy-start.4 = (f32[96]{0:T(128)S(1)}, f32[96]{0:T(128)}, u32[]{:S(2)}) copy-start(f32[96]{0:T(128)} %param.24) | copy-start | bytes 1156
  3.8 2.4 %copy-start.3 = (f32[96]{0:T(128)S(1)}, f32[96]{0:T(128)}, u32[]{:S(2)}) copy-start(f32[96]{0:T(128)} %param.23) | copy-start | bytes 1156
  3.8 2.5 %copy-start.8 = (bf16[1,128,1536]{2,1,0:T(8,128)(2,1)S(1)}, bf16[1,128,1536]{2,1,0:T(8,128)(2,1)}, u32[]{:S(2)}) copy-start(bf16[1,128,1536]{2,1,0:T(8,128)(2,1)} %param.19) | copy-start | bytes 1179652
  3.8 4.7 %copy-start.10 = (bf16[1,128,32]{1,2,0:T(8,128)(2,1)S(1)}, bf16[1,128,32]{1,2,0:T(8,128)(2,1)}, u32[]{:S(2)}) copy-start(bf16[1,128,32]{1,2,0:T(8,128)(2,1)} %param.21) | copy-start | bytes 24580
  5.0 3.8 %copy-start.9 = (bf16[1,128,256]{2,1,0:T(8,128)(2,1)S(1)}, bf16[1,128,256]{2,1,0:T(8,128)(2,1)}, u32[]{:S(2)}) copy-start(bf16[1,128,256]{2,1,0:T(8,128)(2,1)} %param.20) | copy-start | bytes 196612
  5.0 3.8 %copy-start.1 = (bf16[1,128,2048]{2,1,0:T(8,128)(2,1)S(1)}, bf16[1,128,2048]{2,1,0:T(8,128)(2,1)}, u32[]{:S(2)}) copy-start(bf16[1,128,2048]{2,1,0:T(8,128)(2,1)} %param.18) | copy-start | bytes 1572868
  5.0 3.8 %copy-start.5 = (f32[2048]{0:T(1024)S(1)}, f32[2048]{0:T(1024)}, u32[]{:S(2)}) copy-start(f32[2048]{0:T(1024)} %param.29) | copy-start | bytes 24580
  5.0 3.8 %copy-start.6 = (f32[1024]{0:T(1024)S(1)}, f32[1024]{0:T(1024)}, u32[]{:S(2)}) copy-start(f32[1024]{0:T(1024)} %param.27) | copy-start | bytes 12292
  5.0 3.8 %copy-start.7 = (f32[256]{0:T(256)S(1)}, f32[256]{0:T(256)}, u32[]{:S(2)}) copy-start(f32[256]{0:T(256)} %param.22) | copy-start | bytes 3076
  8.8 55.1 %copy-start.12 = (s32[1,128,2]{1,2,0:T(2,128)S(1)}, s32[1,128,2]{1,2,0:T(2,128)}, u32[]{:S(2)}) copy-start(s32[1,128,2]{1,2,0:T(2,128)} %param.30) | copy-start | bytes 3076
  8.9 56.0 %copy-start.11 = (f32[1,128,2]{1,2,0:T(2,128)S(1)}, f32[1,128,2]{1,2,0:T(2,128)}, u32[]{:S(2)}) copy-start(f32[1,128,2]{1,2,0:T(2,128)} %param.32) | copy-start | bytes 3076
  8.9 56.1 %copy-start.13 = (f32[1,128]{1,0:T(1,128)S(1)}, f32[1,128]{1,0:T(1,128)}, u32[]{:S(2)}) copy-start(f32[1,128]{1,0:T(1,128)} %param.31) | copy-start | bytes 1540
  62.2 1.0 copy-start
  63.1 0.8 copy-start.2
where the time goes:
time: 140 us; the launch traced here: 139 us
  Pallas kernels  123 us (88%)
  local copies, waits for them, and re-layouts  8.67 us (6%)
  other arithmetic  6.49 us (5%)
    pallas_call x1, Pallas kernels, routed(): pl.pallas_call(functools.partial(expert_kernel, n_y, n_dp, cap, rows), ou...  70.2 us
    pallas_call x1, Pallas kernels, attended(): pl.pallas_call(functools.partial(attention_kernel, n_sp, n_y, heads, nope...  53.3 us
    unnamed x33, local copies, waits for them, and re-layouts  4.98 us
    neg x1, other arithmetic, attended(): -sin  3.72 us

commit v1 on v0

--- a/solution.py
+++ b/solution.py
@@ -2,6 +2,7 @@
 
 import jax
 import jax.numpy as jnp
+import numpy as np
 from jax import lax
 from jax.experimental import pallas as pl
 from jax.experimental.pallas import tpu as pltpu
@@ -12,12 +13,6 @@
 
 
 eps = 1e-06
-
-
-def angles(offset, span_count, rope_width):
-    position = (offset + jnp.arange(span_count, dtype=jnp.int32)).astype(jnp.float32)
-    frequency = 10000.0 ** (-2.0 * jnp.arange(rope_width // 2, dtype=jnp.float32) / rope_width)
-    return position[:, None] * frequency[None, :]
 
 
 def dot32(a, b):
@@ -211,36 +206,41 @@
 def attention_kernel(
     n_sp,
     n_y,
-    heads,
     nope,
     rope,
     value_width,
-    query_ref,
-    packed_ref,
+    query_hbm,
+    latent_ref,
+    rope_t_ref,
     latent_gain_ref,
-    query_gain_ref,
-    query_swap_ref,
-    key_gain_ref,
-    key_swap_ref,
-    cos_ref,
-    sin_ref,
-    key_weight_ref,
-    value_weight_ref,
-    residual_ref,
+    gains_ref,
+    near_ref,
+    far_ref,
     mix_gain_ref,
     ffn_gain_ref,
+    residual_hbm,
+    key_weight_hbm,
+    value_weight_hbm,
     out_weight_hbm,
     stream_ref,
     normed_ref,
+    residual_ref,
+    key_weight_ref,
+    value_weight_ref,
     out_weight_ref,
+    wide_key,
+    pick_query,
+    turn_query,
     queries_in,
+    packed,
     packed_in,
     queries,
     keys,
     values,
+    bias,
+    weights,
     heads_out,
     token_in,
-    mixed,
     w_sem,
     sq,
     rq,
@@ -252,15 +252,36 @@
     ro,
 ):
     bf = jnp.bfloat16
-    tok = residual_ref.shape[0]
-    length = n_sp * tok
+    f32 = jnp.float32
+    tok = latent_ref.shape[0]
+    lat = latent_ref.shape[1]
     qk = nope + rope
-    lat = packed_ref.shape[1]
+    half = rope // 2
+    n_z = n_sp // n_y
+    heads = n_z
+    slot = 128
+    wide_q = heads * qk
+    wide_v = heads * value_width
     me = lax.axis_index("sp")
-    plane = me // n_y
-    row = me % n_y
-    load = pltpu.make_async_copy(out_weight_hbm, out_weight_ref, w_sem.at[0])
-    load.start()
+    z = me // n_y
+    y = me % n_y
+
+    def local(src, dst, k):
+        return pltpu.make_async_copy(src, dst, w_sem.at[k])
+
+    def query_part(target):
+        return query_hbm.at[:, pl.ds(pl.multiple_of(target * wide_q, slot), wide_q)]
+
+    own_part = pl.ds(pl.multiple_of(z * wide_v, slot), wide_v)
+    loads = [
+        local(key_weight_hbm.at[:, own_part], key_weight_ref, 0),
+        local(value_weight_hbm.at[:, own_part], value_weight_ref, 1),
+        local(query_part(z), queries_in.at[z], 2),
+        local(residual_hbm, residual_ref, 3),
+        local(out_weight_hbm, out_weight_ref, 4),
+    ]
+    for load in loads:
+        load.start()
 
     def remote(src, dst, send, recv, target):
         return pltpu.make_async_remote_copy(
@@ -272,178 +293,226 @@
             device_id_type=pl.DeviceIdType.MESH,
         )
 
+    def at_z(k):
+        return ((z + k) % n_z) * n_y + y
+
+    def at_y(m):
+        return z * n_y + (y + m) % n_y
+
     barrier = pltpu.get_barrier_semaphore()
-    for j in range(1, n_sp):
+    for target in [at_z(k) for k in range(1, n_z)] + [at_y(m) for m in range(1, n_y)]:
         pl.semaphore_signal(
-            barrier,
-            inc=1,
-            device_id={"sp": (me + j) % n_sp},
-            device_id_type=pl.DeviceIdType.MESH,
+            barrier, inc=1, device_id={"sp": target}, device_id_type=pl.DeviceIdType.MESH
         )
-    pl.semaphore_wait(barrier, n_sp - 1)
-
-    down = []
-    for k in range(1, GROUPS):
-        target = ((plane + k) % GROUPS) * n_y + row
-        down.append(remote(packed_ref, packed_in.at[me], sz.at[k], rz.at[k], target))
-        down[-1].start()
-    across = []
+    raw = latent_ref[...].astype(f32)
+    scale = lax.rsqrt(jnp.mean(raw * raw, axis=-1, keepdims=True) + eps)
+    packed[:tok] = (raw * scale * latent_gain_ref[...]).astype(bf)
+    packed[tok:, :tok] = rope_t_ref[:half]
+    packed[tok:, tok:] = rope_t_ref[half:]
+    pl.semaphore_wait(barrier, n_z - 1 + n_y - 1)
+
+    sent = []
+    down = {}
+    for k in (1, 3, 2):
+        down[k] = remote(packed, packed_in.at[me], sz.at[k], rz.at[k], at_z(k))
+        down[k].start()
 
     def spread(k, source):
-        index = ((plane + GROUPS - k) % GROUPS) * n_y + row
-        for m in range(1, n_y):
-            target = plane * n_y + (row + m) % n_y
-            across.append(remote(source, packed_in.at[index], sy.at[k, m], ry.at[k, m], target))
-            across[-1].start()
-
-    spread(0, packed_ref)
-    sent = []
-    for j in range(1, n_sp):
-        target = (me + j) % n_sp
-        sent.append(remote(query_ref.at[target], queries_in.at[me], sq.at[j], rq.at[j], target))
-        sent[-1].start()
-    packed_in[me] = packed_ref[...]
-    queries_in[me] = query_ref[me]
-    for k in range(1, GROUPS):
-        down[k - 1].wait_recv()
-        spread(k, packed_in.at[((plane + GROUPS - k) % GROUPS) * n_y + row])
-    for copy in across:
-        copy.wait_recv()
+        index = ((z + n_z - k) % n_z) * n_y + y
+        for m in (1, 3, 2):
+            sent.append(remote(source, packed_in.at[index], sy.at[k, m], ry.at[k, m], at_y(m)))
+            sent[-1].start()
+
+    spread(0, packed)
+    asked = []
+    for k in (1, 3, 2):
+        target = (z + k) % n_z
+        asked.append(remote(query_part(target), queries_in.at[z], sq.at[k], rq.at[k], at_z(k)))
+        asked[-1].start()
+
+    packed_in[me] = packed[...]
 
     def selector(rows, columns, source):
         i = lax.broadcasted_iota(jnp.int32, (rows, columns), 0)
         c = lax.broadcasted_iota(jnp.int32, (rows, columns), 1)
-        return (i == source(c)).astype(jnp.float32).astype(bf)
-
-    half = rope // 2
+        return (i == source(c // slot, c % slot)).astype(f32).astype(bf)
 
     def swapped(c):
-        return jnp.where(c < nope, -1, jnp.where(c < nope + half, c + half, c - half))
-
-    def shape_head(plain, turned, gain, swap_gain, rows):
-        scale = lax.rsqrt(jnp.sum(plain * plain, axis=-1, keepdims=True) / qk + eps)
+        return jnp.where(
+            c < nope, -1, jnp.where(c < nope + half, c + half, jnp.where(c < qk, c - half, -1))
+        )
+
+    def plain_of(c, first):
+        return jnp.where((c >= first) & (c < qk), c, -1)
+
+    pick_query[...] = selector(
+        wide_q, heads * slot, lambda h, c: jnp.where(c < qk, c + h * qk, -1)
+    )
+    turn_query[...] = selector(
+        wide_q,
+        heads * slot,
+        lambda h, c: jnp.where((c >= nope) & (c < qk), swapped(c) + h * qk, -1),
+    )
+    pick_rope = selector(
+        rope,
+        2 * slot,
+        lambda h, c: jnp.where(
+            (c < nope) | (c >= qk), -1, jnp.where(h == 0, c, swapped(c)) - nope
+        ),
+    )
+    q_pos = y * tok + lax.broadcasted_iota(jnp.int32, bias.shape, 0)
+    k_pos = lax.broadcasted_iota(jnp.int32, bias.shape, 1)
+    bias[...] = jnp.where(k_pos // SPAN <= q_pos // SPAN, 0.0, -1e30)
+    loads[0].wait()
+    wide_key[...] = dot32(
+        key_weight_ref[...],
+        selector(heads * nope, heads * slot, lambda h, c: jnp.where(c < nope, c + h * nope, -1)),
+    ).astype(bf)
+    loads[1].wait()
+
+    for k in (1, 3, 2):
+        down[k].wait_recv()
+        spread(k, packed_in.at[((z + n_z - k) % n_z) * n_y + y])
+
+    near_cos, near_sin = near_ref[0], near_ref[1]
+
+    def tables(block):
+        far_cos = far_ref[0, pl.ds(block, 1), :]
+        far_sin = far_ref[1, pl.ds(block, 1), :]
         return (
-            plain * scale * gain * cos_ref[rows, :] + turned * scale * swap_gain * sin_ref[rows, :]
-        ).astype(bf)
-
-    strips = lat // rope
-    strip_rows = tok // strips
-
-    def prepare(s, carry):
+            far_cos * near_cos - far_sin * near_sin,
+            far_sin * near_cos + far_cos * near_sin,
+        )
+
+    query_gain, query_swap = gains_ref[0:1, :], gains_ref[1:2, :]
+    key_gain, key_swap = gains_ref[2:3, :], gains_ref[3:4, :]
+
+    def prepare(i, carry):
+        step = i // n_y
+        k = jnp.where(step < 2, step, 5 - step)
+        m = i % n_y
+        origin = (z + n_z - k) % n_z
+        s = origin * n_y + (y + n_y - m) % n_y
+
+        @pl.when(m > 0)
+        def _():
+            remote(packed, packed_in.at[s], sy.at[k, m], ry.at[k, m], me).wait_recv()
+
         rows = pl.ds(pl.multiple_of(s * tok, tok), tok)
         block = packed_in[s]
-        raw = block[:tok].astype(jnp.float32)
-        scale = lax.rsqrt(jnp.mean(raw * raw, axis=-1, keepdims=True) + eps)
-        latent = (raw * scale * latent_gain_ref[...]).astype(bf)
+        latent = block[:tok]
         values[rows, :] = dot32(latent, value_weight_ref[...]).astype(bf)
-        part = dot32(latent, key_weight_ref[...]).astype(bf)
-        tail = block[tok:]
-        plain_rope = jnp.concatenate(
-            [
-                dot32(tail, selector(lat, qk, lambda c: jnp.where(c < nope, -1, c - nope + i * rope)))
-                for i in range(strips)
-            ],
-            axis=0,
-        )
-        turned = jnp.concatenate(
-            [
-                dot32(
-                    tail,
-                    selector(
-                        lat, qk, lambda c: jnp.where(c < nope, -1, swapped(c) - nope + i * rope)
-                    ),
-                )
-                for i in range(strips)
-            ],
-            axis=0,
-        )
+        part = dot32(latent, wide_key[...]).astype(bf).astype(f32)
+        turned_rows = jnp.concatenate([block[tok:, :tok], block[tok:, tok:]], axis=0)
+        spun = dot_t(turned_rows, pick_rope)
+        cos, sin = tables(s)
+        plain_rope = spun[:, :slot]
+        tail = plain_rope * (key_gain * cos) + spun[:, slot:] * (key_swap * sin)
         for h in range(heads):
-            plain = plain_rope + dot32(
-                part, selector(heads * nope, qk, lambda c: jnp.where(c < nope, c + h * nope, -1))
-            )
-            keys[h, rows, :] = shape_head(
-                plain, turned, key_gain_ref[...], key_swap_ref[...], rows
-            )
+            own = part[:, h * slot : (h + 1) * slot]
+            full = own + plain_rope
+            norm = lax.rsqrt(jnp.sum(full * full, axis=-1, keepdims=True) / qk + eps)
+            keys[h, rows, :] = ((own * key_gain + tail) * norm).astype(bf)
         return carry
 
     lax.fori_loop(0, n_sp, prepare, 0)
-    for copy in sent:
+
+    loads[2].wait()
+    for copy in asked:
         copy.wait_recv()
 
-    def prepare_queries(s, carry):
-        rows = pl.ds(pl.multiple_of(s * tok, tok), tok)
-        raw = queries_in[s]
+    def prepare_queries(b, carry):
+        raw = queries_in[b]
+        plain = dot32(raw, pick_query[...])
+        turned = dot32(raw, turn_query[...])
+        cos, sin = tables(b * n_y + y)
         for h in range(heads):
-            plain = dot32(raw, selector(heads * qk, qk, lambda c: c + h * qk))
-            turned = dot32(
-                raw,
-                selector(
-                    heads * qk, qk, lambda c: jnp.where(c < nope, -1, swapped(c) + h * qk)
-                ),
-            )
-            queries[h, rows, :] = shape_head(
-                plain, turned, query_gain_ref[...], query_swap_ref[...], rows
-            )
+            span = slice(h * slot, (h + 1) * slot)
+            own = plain[:, span]
+            norm = lax.rsqrt(jnp.sum(own * own, axis=-1, keepdims=True) / qk + eps)
+            queries[b, h] = (
+                (own * (query_gain * cos) + turned[:, span] * (query_swap * sin)) * norm
+            ).astype(bf)
         return carry
 
-    lax.fori_loop(0, n_sp, prepare_queries, 0)
-
-    blocks = 4
-    block_rows = length // blocks
-    for b in range(blocks):
-        first_row = b * block_rows
-        last_row = first_row + block_rows
-        total = None
-        lane = lax.broadcasted_iota(jnp.int32, (block_rows, heads * value_width), 1)
-        q_pos = first_row + lax.broadcasted_iota(jnp.int32, (block_rows, last_row), 0)
-        k_pos = lax.broadcasted_iota(jnp.int32, (block_rows, last_row), 1)
-        allowed = k_pos // SPAN <= q_pos // SPAN
+    lax.fori_loop(0, n_z, prepare_queries, 0)
+
+    stretch = n_y * tok
+    factor = qk ** (-0.5) * 1.4426950408889634
+    lane = lax.broadcasted_iota(jnp.int32, (tok, wide_v), 1) // value_width
+    for b in range(n_z - 1, -1, -1):
+        last = (b + 1) * stretch
+        sums = []
         for h in range(heads):
             scores = lax.dot_general(
-                queries[h, first_row:last_row],
-                keys[h, :last_row],
+                queries[b, h],
+                keys[h, :last],
                 (((1,), (1,)), ((), ())),
-                preferred_element_type=jnp.float32,
-            ) * (qk ** (-0.5))
-            scores = jnp.where(allowed, scores, -1e30)
-            raised = jnp.exp(scores - jnp.max(scores, axis=-1, keepdims=True))
-            row_sum = jnp.sum(raised, axis=-1, keepdims=True)
-            mine = dot32(raised.astype(bf), values[:last_row]) / row_sum
-            total = mine if total is None else jnp.where(lane < h * value_width, total, mine)
-        total = total.astype(bf)
-        for t in range(block_rows // tok):
-            index = first_row // tok + t
-            heads_out[index] = total[t * tok : (t + 1) * tok]
-
-            @pl.when(index != me)
-            def _():
-                remote(
-                    heads_out.at[index], token_in.at[me], so.at[index], ro.at[me], index
-                ).start()
-
-    token_in[me] = heads_out[me]
-    load.wait()
-    for j in range(1, n_sp):
-        other = (me + j) % n_sp
+                preferred_element_type=f32,
+            )
+            edge = scores[:, last - stretch :] + bias[...]
+            top = jnp.max(edge, axis=-1, keepdims=True)
+            if b:
+                inner = scores[:, : last - stretch]
+                top = jnp.maximum(top, jnp.max(inner, axis=-1, keepdims=True))
+            raised = jnp.exp2((edge - top) * factor)
+            total = jnp.sum(raised, axis=-1, keepdims=True)
+            weights[h * tok : (h + 1) * tok, last - stretch : last] = raised.astype(bf)
+            if b:
+                raised = jnp.exp2((inner - top) * factor)
+                total = total + jnp.sum(raised, axis=-1, keepdims=True)
+                weights[h * tok : (h + 1) * tok, : last - stretch] = raised.astype(bf)
+            sums.append(total)
+        mixed = dot32(weights[:, :last], values[:last])
+        total = None
+        for h in range(heads):
+            mine = mixed[h * tok : (h + 1) * tok] / sums[h]
+            total = mine if total is None else jnp.where(lane < h, total, mine)
+        heads_out[b] = total.astype(bf)
+
+        @pl.when(z != b)
+        def _():
+            remote(
+                heads_out.at[b], token_in.at[z], so.at[b], ro.at[z], b * n_y + y
+            ).start()
+
+    token_in[z] = heads_out[z]
+    loads[3].wait()
+    loads[4].wait()
+    for k in range(1, n_z):
+        other = (z + k) % n_z
         remote(
-            heads_out.at[other], token_in.at[other], so.at[other], ro.at[other], other
+            heads_out.at[other], token_in.at[other], so.at[other], ro.at[other], other * n_y + y
         ).wait()
-    wide = heads * value_width
     square = None
-    for s in range(n_sp):
-        piece = token_in[s].astype(jnp.float32)
+    for s in range(n_z):
+        piece = token_in[s].astype(f32)
         part = jnp.sum(piece * piece, axis=-1, keepdims=True)
         square = part if square is None else square + part
-    scale = lax.rsqrt(square / (n_sp * wide) + eps)
-    for s in range(n_sp):
-        span = slice(s * wide, (s + 1) * wide)
-        mixed[:, span] = (token_in[s].astype(jnp.float32) * scale * mix_gain_ref[:, span]).astype(bf)
-    stream = residual_ref[...].astype(jnp.float32) + dot32(mixed[...], out_weight_ref[...])
+    scale = lax.rsqrt(square / (n_z * wide_v) + eps)
+    mixed = jnp.concatenate(
+        [
+            (token_in[s].astype(f32) * scale * mix_gain_ref[:, s * wide_v : (s + 1) * wide_v]).astype(bf)
+            for s in range(n_z)
+        ],
+        axis=1,
+    )
+    stream = residual_ref[...].astype(f32) + dot32(mixed, out_weight_ref[...])
     stream_ref[...] = stream
     scale = lax.rsqrt(jnp.mean(stream * stream, axis=-1, keepdims=True) + eps)
     normed_ref[...] = (stream * scale * ffn_gain_ref[...]).astype(bf)
-    for copy in down + across + sent:
+    for copy in list(down.values()) + sent + asked:
         copy.wait_send()
+
+
+def trig(positions, nope, rope):
+    frequency = 10000.0 ** (-2.0 * np.arange(rope // 2) / rope)
+    angle = np.asarray(positions, np.float64)[:, None] * frequency[None, :]
+    cos = np.ones((len(positions), 128))
+    sin = np.zeros((len(positions), 128))
+    cos[:, nope : nope + rope] = np.concatenate([np.cos(angle)] * 2, axis=1)
+    sin[:, nope : nope + rope] = np.concatenate([np.sin(angle)] * 2, axis=1)
+    return np.stack([cos, sin]).astype(np.float32)
 
 
 def attended(
@@ -465,78 +534,80 @@
 ):
     n_sp = lax.axis_size("sp")
     n_y = n_sp // GROUPS
-    me = lax.axis_index("sp")
+    n_z = GROUPS
     tok, width = residual.shape
     rope = rope_key.shape[1]
     qk = nope + rope
     lat = latent.shape[1]
-    heads = head_count // n_sp
+    heads = head_count // n_z
     length = n_sp * tok
     half = rope // 2
     bf = jnp.bfloat16
-    query_blocks = query.reshape(tok, n_sp, heads * qk).transpose(1, 0, 2)
-    strips = lat // rope
-    tail = rope_key.reshape(strips, tok // strips, rope).transpose(1, 0, 2).reshape(-1, lat)
-    packed = jnp.concatenate([latent, tail], axis=0)
-    phases = angles(0, length, rope)
-    cos, sin = jnp.cos(phases), jnp.sin(phases)
-    cos = jnp.concatenate([jnp.ones((length, nope), jnp.float32), cos, cos], axis=1)
-    sin = jnp.concatenate([jnp.zeros((length, nope), jnp.float32), -sin, sin], axis=1)
-
-    def swap(gain):
-        return jnp.concatenate([gain[:nope], gain[nope + half :], gain[nope : nope + half]])
-
-    key_own = lax.dynamic_slice_in_dim(key_weight, me * heads * nope, heads * nope, 1)
-    value_own = lax.dynamic_slice_in_dim(value_weight, me * heads * value_width, heads * value_width, 1)
+    slot = 128
+
+    def both(gain):
+        turned = jnp.concatenate([jnp.zeros((nope,)), -gain[nope + half :], gain[nope : nope + half]])
+        return jnp.pad(jnp.stack([gain, turned]), ((0, 0), (0, slot - qk)))
+
+    gains = jnp.concatenate([both(query_gain), both(key_gain)], axis=0)
+    near = jnp.asarray(trig(np.arange(tok), nope, rope))
+    far = jnp.asarray(trig(np.arange(n_sp) * tok, nope, rope))
     vmem = pl.BlockSpec(memory_space=pltpu.VMEM)
+    hbm = pl.BlockSpec(memory_space=pl.ANY)
     dma = pltpu.SemaphoreType.DMA
-    wide = heads * value_width
+    wide_v = heads * value_width
     return pl.pallas_call(
-        functools.partial(attention_kernel, n_sp, n_y, heads, nope, rope, value_width),
+        functools.partial(attention_kernel, n_sp, n_y, nope, rope, value_width),
         out_shape=(
             jax.ShapeDtypeStruct((tok, width), jnp.float32),
             jax.ShapeDtypeStruct((tok, width), bf),
         ),
-        in_specs=[vmem] * 14 + [pl.BlockSpec(memory_space=pl.ANY)],
+        in_specs=[hbm] + [vmem] * 8 + [hbm] * 4,
         out_specs=(vmem, vmem),
         scratch_shapes=[
+            pltpu.VMEM((tok, width), bf),
+            pltpu.VMEM((lat, wide_v), bf),
+            pltpu.VMEM((lat, wide_v), bf),
             pltpu.VMEM(out_weight.shape, bf),
-            pltpu.VMEM((n_sp, tok, heads * qk), bf),
-            pltpu.VMEM((n_sp,) + packed.shape, bf),
-            pltpu.VMEM((heads, length, qk), bf),
-            pltpu.VMEM((heads, length, qk), bf),
-            pltpu.VMEM((length, wide), bf),
-            pltpu.VMEM((n_sp, tok, wide), bf),
-            pltpu.VMEM((n_sp, tok, wide), bf),
-            pltpu.VMEM((tok, n_sp * wide), bf),
-            dma((1,)),
-            dma((n_sp,)),
-            dma((n_sp,)),
-            dma((GROUPS,)),
-            dma((GROUPS,)),
-            dma((GROUPS, n_y)),
-            dma((GROUPS, n_y)),
-            dma((n_sp,)),
-            dma((n_sp,)),
+            pltpu.VMEM((lat, heads * slot), bf),
+            pltpu.VMEM((heads * qk, heads * slot), bf),
+            pltpu.VMEM((heads * qk, heads * slot), bf),
+            pltpu.VMEM((n_z, tok, heads * qk), bf),
+            pltpu.VMEM((tok + half, lat), bf),
+            pltpu.VMEM((n_sp, tok + half, lat), bf),
+            pltpu.VMEM((n_z, heads, tok, slot), bf),
+            pltpu.VMEM((heads, length, slot), bf),
+            pltpu.VMEM((length, wide_v), bf),
+            pltpu.VMEM((tok, n_y * tok), jnp.float32),
+            pltpu.VMEM((heads * tok, length), bf),
+            pltpu.VMEM((n_z, tok, wide_v), bf),
+            pltpu.VMEM((n_z, tok, wide_v), bf),
+            dma((5,)),
+            dma((n_z,)),
+            dma((n_z,)),
+            dma((n_z,)),
+            dma((n_z,)),
+            dma((n_z, n_y)),
+            dma((n_z, n_y)),
+            dma((n_z,)),
+            dma((n_z,)),
         ],
         compiler_params=pltpu.CompilerParams(
             collective_id=1, has_side_effects=True, vmem_limit_bytes=48 * 1024 * 1024
         ),
     )(
-        query_blocks,
-        packed,
+        query,
+        latent,
+        rope_key.T,
         latent_gain[None],
-        query_gain[None],
-        swap(query_gain)[None],
-        key_gain[None],
-        swap(key_gain)[None],
-        cos,
-        sin,
-        key_own,
-        value_own,
-        residual,
+        gains,
+        near,
+        far,
         mix_gain[None],
         ffn_gain[None],
+        residual,
+        key_weight,
+        value_weight,
         out_weight,
     )
 

time: 140 us -> 125 us (0.89)
  Pallas kernels: 123 us -> 103 us
  local copies, waits for them, and re-layouts: 8.67 us -> 15.6 us
    pallas_call x1, Pallas kernels: 53.3 us -> 34.9 us  [attended(): pl.pallas_call(functools.partial(attention_kernel, n_sp, n_y, nope, rope,...]
    unnamed x33 -> x29, local copies, waits for them, and re-layouts: 4.98 us -> 14.5 us
    neg x1 -> x2, other arithmetic: 3.72 us -> 1.6 us  [both(): -gain[nope + half:]]
    pallas_call x1, Pallas kernels: 70.2 us -> 68.3 us  [routed(): pl.pallas_call(functools.partial(expert_kernel, n_y, n_dp, cap, rows), ou...]
    another operation x2 -> x4, other arithmetic: 0.11 us -> 1.52 us
where the time goes in v1:
time: 125 us; the launch traced here: 124 us
  Pallas kernels  103 us (82%)
  local copies, waits for them, and re-layouts  15.6 us (12%)
  other arithmetic  5.25 us (4%)
    pallas_call x1, Pallas kernels, routed(): pl.pallas_call(functools.partial(expert_kernel, n_y, n_dp, cap, rows), ou...  68.3 us
    pallas_call x1, Pallas kernels, attended(): pl.pallas_call(functools.partial(attention_kernel, n_sp, n_y, nope, rope,...  34.9 us
    unnamed x29, local copies, waits for them, and re-layouts  14.5 us

profile of v1, /device:TPU:0, one launch (start us, length us, event | category | flops | bytes accessed | tf_op | source)
XLA Modules:
  0.0 124.2 jit_solution(14134587951874930148)
XLA Ops:
  0.0 0.7 reduce_sum.28
  0.7 0.8 slice_negate_fusion.1
  1.5 0.8 slice_negate_fusion
  2.3 0.1 fusion.7
  2.4 0.7 select_maximum_fusion
  3.1 0.8 copy.31
  3.9 0.1 copy.33
  4.0 0.2 convert_reduce_fusion
  4.2 0.2 fusion.8
  4.3 0.1 subtract_multiply_fusion
  4.4 0.1 copy.35
  4.5 0.2 convert_reduce_fusion.1
  4.7 0.1 copy.37
  4.9 0.7 compare_convert_fusion.pick_ref
  5.6 0.8 copy.36
  6.4 0.8 fusion
  7.1 0.1 fusion.9
  7.2 0.7 concatenate.16.info_ref
  8.0 0.0 copy-start.1
  8.0 1.0 copy-done.1
  9.0 0.0 copy-start.2
  9.0 1.0 copy-done.2
  10.1 0.0 copy-start.3
  10.1 1.0 copy-done.3
  11.1 0.0 copy-start.5
  11.1 1.0 copy-done.5
  12.1 0.0 copy-start.6
  12.1 0.9 copy-done.6
  13.0 0.0 copy-start.7
  13.0 0.8 copy-done.7
  13.8 0.0 copy-start.8
  13.8 0.7 copy-done.8
  14.6 0.0 copy-start.9
  14.6 0.7 copy-done.9
  15.3 0.0 copy-start.10
  15.3 0.7 copy-done.10
  16.0 0.0 copy-start.11
  16.0 0.7 copy-done.11
  16.6 0.0 copy-start.12
  16.6 0.7 copy-done.12
  17.3 34.9 %shard_map.190 = (f32[128,2048]{1,0:T(8,128)S(1)}, bf16[128,2048]{1,0:T(8,128)(2,1)S(1)}) custom-call(bf16[128,1536]{1,0:T(8,128)(2,1)S(1)} %bitcast.31, bf16[128,256]{1,0:T(8,128)(2,1)S(1)} %bitcast.32, bf16[32,128]{1,0:T(8,128)(2,1)S(1)} %bitcast.33, f32[1,256]{1,0:T(1,128)S(1)} %bitcast.36, f32[4,128]{1,0:T(4,128)S(1)} %pad_maximum_fusion.gains_ref, ...), custom_call_target="tpu_custom_call" | custom-call | tf_op jit(solution)/shard_map/pallas_call | solution.py:559
  52.2 0.0 copy-start
  52.3 1.0 copy-done
  53.2 0.0 copy-start.4
  53.2 0.8 copy-done.4
  54.0 68.3 %shard_map.191 = bf16[128,2048]{1,0:T(8,128)(2,1)} custom-call(bf16[128,2048]{1,0:T(8,128)(2,1)} %copy-done.4, bf16[128,128]{1,0:T(8,128)(2,1)} %concatenate.16.info_ref, bf16[4,64,128]{2,1,0:T(8,128)(2,1)} %compare_convert_fusion.pick_ref, f32[128,2048]{1,0:T(8,128)} %copy-done, bf16[2048,512]{1,0:T(8,128)(2,1)} %bitcast.38, bf16[2048,512]{1,0:T(8,128)(2,1)} %bitcast.39, ...), custom_call_target="tpu_custom_call" | custom-call | tf_op jit(solution)/shard_map/pallas_call | solution.py:655
  122.3 1.9 %copy.39 = bf16[1,128,2048]{2,1,0:T(8,128)(2,1)} copy(bf16[1,128,2048]{2,1,0:T(8,128)(2,1)} %bitcast.37) | data formatting | bytes 1048576
  (8 shorter events, 0.1 us)
Async XLA Ops:
  8.0 1.0 copy-start.1
  9.0 1.0 copy-start.2
  10.1 1.0 copy-start.3
  11.1 1.0 copy-start.5
  12.1 0.9 copy-start.6
  13.0 0.8 copy-start.7
  13.8 0.7 copy-start.8
  14.6 0.7 copy-start.9
  15.3 0.7 copy-start.10
  16.0 0.7 copy-start.11
  16.6 0.7 copy-start.12
  52.2 1.0 copy-start
  53.2 0.8 copy-start.4

commit v2 on v1

v2 whole, which is shorter than its diff:
```python
import functools

import jax
import jax.numpy as jnp
import numpy as np
from jax import lax
from jax.experimental import pallas as pl
from jax.experimental.pallas import tpu as pltpu
from jax.sharding import PartitionSpec as P

GROUPS = 4
SPAN = 64


eps = 1e-06


def dot32(a, b):
    return jnp.dot(a, b, preferred_element_type=jnp.float32)


def dot_t(a, b):
    return lax.dot_general(a, b, (((0,), (0,)), ((), ())), preferred_element_type=jnp.float32)


def layer_kernel(
    n_sp,
    n_y,
    n_dp,
    nope,
    rope,
    value_width,
    cap,
    top,
    residual_hbm,
    query_hbm,
    latent_hbm,
    rope_t_hbm,
    latent_gain_hbm,
    query_gain_hbm,
    key_gain_hbm,
    key_weight_hbm,
    value_weight_hbm,
    mix_gain_hbm,
    out_weight_hbm,
    ffn_gain_hbm,
    choice_hbm,
    group_prob_hbm,
    share_hbm,
    gate_hbm,
    up_hbm,
    down_hbm,
    near_hbm,
    far_hbm,
    out_ref,
    residual_ref,
    latent_ref,
    rope_t_ref,
    latent_gain_ref,
    query_gain_ref,
    key_gain_ref,
    key_weight_ref,
    value_weight_ref,
    mix_gain_ref,
    out_weight_ref,
    ffn_gain_ref,
    choice_ref,
    group_prob_ref,
    share_ref,
    gate_ref,
    up_ref,
    down_ref,
    near_ref,
    far_ref,
    wide_key,
    pick_query,
    turn_query,
    queries_in,
    packed,
    packed_in,
    queries,
    keys,
    values,
    bias,
    weights,
    heads_out,
    token_in,
    normed_ref,
    info_ref,
    pick_ref,
    out1,
    in1,
    out2,
    arrive,
    served,
    back2,
    merged,
    home,
    acc,
    w_sem,
    sq,
    rq,
    sz,
    rz,
    sy,
    ry,
    so,
    ro,
    s1,
    r1,
    s2,
    r2,
    s3,
    r3,
    s4,
    r4,
):
    bf = jnp.bfloat16
    f32 = jnp.float32
    tok = latent_ref.shape[0]
    width = out_ref.shape[1]
    qk = nope + rope
    half = rope // 2
    n_z = n_sp // n_y
    heads = n_z
    slot = 128
    wide_q = heads * qk
    wide_v = heads * value_width
    me = lax.axis_index("sp")
    z = me // n_y
    y = me % n_y

    def query_part(target):
        return query_hbm.at[:, pl.ds(pl.multiple_of(target * wide_q, slot), wide_q)]

    own_part = pl.ds(pl.multiple_of(z * wide_v, slot), wide_v)
    pairs = [
        (latent_hbm, latent_ref),
        (latent_gain_hbm, latent_gain_ref),
        (rope_t_hbm, rope_t_ref),
        (key_weight_hbm.at[:, own_part], key_weight_ref),
        (value_weight_hbm.at[:, own_part], value_weight_ref),
        (near_hbm, near_ref),
        (far_hbm, far_ref),
        (query_gain_hbm, query_gain_ref),
        (key_gain_hbm, key_gain_ref),
        (query_part(z), queries_in.at[z]),
        (choice_hbm, choice_ref),
        (group_prob_hbm, group_prob_ref),
        (share_hbm, share_ref),
        (mix_gain_hbm, mix_gain_ref),
        (ffn_gain_hbm, ffn_gain_ref),
        (residual_hbm, residual_ref),
        (out_weight_hbm, out_weight_ref),
        (gate_hbm, gate_ref),
        (up_hbm, up_ref),
        (down_hbm, down_ref),
    ]
    loads = [
        pltpu.make_async_copy(src, dst, w_sem.at[n]) for n, (src, dst) in enumerate(pairs)
    ]
    small = 15
    for load in loads[:small]:
        load.start()

    def remote(src, dst, send, recv, target):
        return pltpu.make_async_remote_copy(
            src_ref=src,
            dst_ref=dst,
            send_sem=send,
            recv_sem=recv,
            device_id=target if isinstance(target, dict) else {"sp": target},
            device_id_type=pl.DeviceIdType.MESH,
        )

    dp = lax.axis_index("dp")
    peers = n_y * n_dp
    rows = tok // top
    mine = y * n_dp + dp

    def peer(j):
        other = (mine + j) % peers
        return {"sp": z * n_y + other // n_dp, "dp": other % n_dp}

    def at_z(k):
        return ((z + k) % n_z) * n_y + y

    def at_y(m):
        return z * n_y + (y + m) % n_y

    barrier = pltpu.get_barrier_semaphore()
    for target in [{"sp": at_z(k)} for k in range(1, n_z)] + [peer(j) for j in range(1, peers)]:
        pl.semaphore_signal(
            barrier, inc=1, device_id=target, device_id_type=pl.DeviceIdType.MESH
        )
    for load in loads[:3]:
        load.wait()
    raw = latent_ref[...].astype(f32)
    scale = lax.rsqrt(jnp.mean(raw * raw, axis=-1, keepdims=True) + eps)
    packed[:tok] = (raw * scale * latent_gain_ref[...]).astype(bf)
    packed[tok:, :tok] = rope_t_ref[:half]
    packed[tok:, tok:] = rope_t_ref[half:]
    pl.semaphore_wait(barrier, n_z - 1 + peers - 1)

    sent = []
    down = {}
    for k in (1, 3, 2):
        down[k] = remote(packed, packed_in.at[me], sz.at[k], rz.at[k], at_z(k))
        down[k].start()

    def spread(k, source):
        index = ((z + n_z - k) % n_z) * n_y + y
        for m in (1, 3, 2):
            sent.append(remote(source, packed_in.at[index], sy.at[k, m], ry.at[k, m], at_y(m)))
            sent[-1].start()

    spread(0, packed)
    asked = []
    for k in (1, 3, 2):
        target = (z + k) % n_z
        asked.append(remote(query_part(target), queries_in.at[z], sq.at[k], rq.at[k], at_z(k)))
        asked[-1].start()

    for load in loads[small:]:
        load.start()
    packed_in[me] = packed[...]

    def selector(rows, columns, source):
        i = lax.broadcasted_iota(jnp.int32, (rows, columns), 0)
        c = lax.broadcasted_iota(jnp.int32, (rows, columns), 1)
        return (i == source(c // slot, c % slot)).astype(f32).astype(bf)

    def swapped(c):
        return jnp.where(
            c < nope, -1, jnp.where(c < nope + half, c + half, jnp.where(c < qk, c - half, -1))
        )

    def plain_of(c, first):
        return jnp.where((c >= first) & (c < qk), c, -1)

    def route():
        lower = lax.broadcasted_iota(jnp.int32, (tok, tok), 0)
        upper = lax.broadcasted_iota(jnp.int32, (tok, tok), 1)
        before = (lower < upper).astype(f32).astype(bf)
        per_group = peers
        chosen = choice_ref[...]
        group = chosen[0:1] // per_group
        of_group = (
            lax.broadcasted_iota(jnp.int32, (8, tok), 0) == jnp.broadcast_to(group, (8, tok))
        ).astype(f32)
        rank = jnp.sum(of_group * dot32(of_group.astype(bf), before), axis=0, keepdims=True)
        line = group * rows + rank.astype(jnp.int32)
        place = lax.broadcasted_iota(jnp.int32, (n_z * rows, tok), 0)
        pick = (place == jnp.broadcast_to(line, place.shape)).astype(f32).astype(bf)
        for g in range(n_z):
            pick_ref[g] = pick[g * rows : (g + 1) * rows]
        expert = lax.broadcasted_iota(jnp.int32, (n_z * per_group, tok), 0)
        of_expert = [
            (expert == jnp.broadcast_to(chosen[t : t + 1], expert.shape)).astype(f32)
            for t in range(top)
        ]
        named = of_expert[0]
        for t in range(1, top):
            named = named + of_expert[t]
        count = dot32(named.astype(bf), before)
        share = share_ref[...]
        whole = share[0:1]
        for t in range(1, top):
            whole = whole + share[t : t + 1]
        lines = []
        for t in range(top):
            earlier = jnp.sum(of_expert[t] * count, axis=0, keepdims=True)
            local_one = ((chosen[t : t + 1] - group * per_group) * cap).astype(f32)
            lines.append(local_one + earlier)
        for t in range(top):
            part = group_prob_ref[...] * share[t : t + 1] / whole
            high = part.astype(bf).astype(f32)
            lines += [high, part - high]
        at = lax.broadcasted_iota(jnp.int32, (slot, tok), 0)
        total = jnp.zeros((slot, tok), f32)
        for n, values_of in enumerate(lines):
            total = jnp.where(at == n, jnp.broadcast_to(values_of, at.shape), total)
        info_ref[...] = total.astype(bf)

    pick_query[...] = selector(
        wide_q, heads * slot, lambda h, c: jnp.where(c < qk, c + h * qk, -1)
    )
    turn_query[...] = selector(
        wide_q,
        heads * slot,
        lambda h, c: jnp.where((c >= nope) & (c < qk), swapped(c) + h * qk, -1),
    )
    pick_rope = selector(
        rope,
        2 * slot,
        lambda h, c: jnp.where(
            (c < nope) | (c >= qk), -1, jnp.where(h == 0, c, swapped(c)) - nope
        ),
    )
    q_pos = y * tok + lax.broadcasted_iota(jnp.int32, bias.shape, 0)
    k_pos = lax.broadcasted_iota(jnp.int32, bias.shape, 1)
    bias[...] = jnp.where(k_pos // SPAN <= q_pos // SPAN, 0.0, -1e30)
    loads[3].wait()
    wide_key[...] = dot32(
        key_weight_ref[...],
        selector(heads * nope, heads * slot, lambda h, c: jnp.where(c < nope, c + h * nope, -1)),
    ).astype(bf)
    for load in loads[4:small]:
        load.wait()
    route()

    for k in (1, 3, 2):
        down[k].wait_recv()
        spread(k, packed_in.at[((z + n_z - k) % n_z) * n_y + y])

    near_cos, near_sin = near_ref[0], near_ref[1]

    def tables(block):
        far_cos = far_ref[0, pl.ds(block, 1), :]
        far_sin = far_ref[1, pl.ds(block, 1), :]
        return (
            far_cos * near_cos - far_sin * near_sin,
            far_sin * near_cos + far_cos * near_sin,
        )

    def both(gain_ref):
        gain = jnp.concatenate([gain_ref[...], jnp.zeros((1, slot - qk), f32)], axis=1)
        gain = jnp.broadcast_to(gain, (8, slot))
        c = lax.broadcasted_iota(jnp.int32, (8, slot), 1)
        up = pltpu.roll(gain, half, 1)
        down_by = pltpu.roll(gain, slot - half, 1)
        turned = jnp.where(
            c < nope, 0.0, jnp.where(c < nope + half, -down_by, jnp.where(c < qk, up, 0.0))
        )
        return gain[0:1], turned[0:1]

    query_gain, query_swap = both(query_gain_ref)
    key_gain, key_swap = both(key_gain_ref)

    def prepare(i, carry):
        step = i // n_y
        k = jnp.where(step < 2, step, 5 - step)
        m = i % n_y
        origin = (z + n_z - k) % n_z
        s = origin * n_y + (y + n_y - m) % n_y

        @pl.when(m > 0)
        def _():
            remote(packed, packed_in.at[s], sy.at[k, m], ry.at[k, m], me).wait_recv()

        at = pl.ds(pl.multiple_of(s * tok, tok), tok)
        block = packed_in[s]
        latent = block[:tok]
        values[at, :] = dot32(latent, value_weight_ref[...]).astype(bf)
        part = dot32(latent, wide_key[...]).astype(bf).astype(f32)
        turned_rows = jnp.concatenate([block[tok:, :tok], block[tok:, tok:]], axis=0)
        spun = dot_t(turned_rows, pick_rope)
        cos, sin = tables(s)
        plain_rope = spun[:, :slot]
        tail = plain_rope * (key_gain * cos) + spun[:, slot:] * (key_swap * sin)
        for h in range(heads):
            own = part[:, h * slot : (h + 1) * slot]
            full = own + plain_rope
            norm = lax.rsqrt(jnp.sum(full * full, axis=-1, keepdims=True) / qk + eps)
            keys[h, at, :] = ((own * key_gain + tail) * norm).astype(bf)
        return carry

    lax.fori_loop(0, n_sp, prepare, 0)

    for copy in asked:
        copy.wait_recv()

    def prepare_queries(b, carry):
        raw = queries_in[b]
        plain = dot32(raw, pick_query[...])
        turned = dot32(raw, turn_query[...])
        cos, sin = tables(b * n_y + y)
        for h in range(heads):
            span = slice(h * slot, (h + 1) * slot)
            own = plain[:, span]
            norm = lax.rsqrt(jnp.sum(own * own, axis=-1, keepdims=True) / qk + eps)
            queries[b, h] = (
                (own * (query_gain * cos) + turned[:, span] * (query_swap * sin)) * norm
            ).astype(bf)
        return carry

    lax.fori_loop(0, n_z, prepare_queries, 0)

    stretch = n_y * tok
    factor = qk ** (-0.5) * 1.4426950408889634
    lane = lax.broadcasted_iota(jnp.int32, (tok, wide_v), 1) // value_width
    for b in range(n_z - 1, -1, -1):
        last = (b + 1) * stretch
        sums = []
        for h in range(heads):
            scores = lax.dot_general(
                queries[b, h],
                keys[h, :last],
                (((1,), (1,)), ((), ())),
                preferred_element_type=f32,
            )
            edge = scores[:, last - stretch :] + bias[...]
            top = jnp.max(edge, axis=-1, keepdims=True)
            if b:
                inner = scores[:, : last - stretch]
                top = jnp.maximum(top, jnp.max(inner, axis=-1, keepdims=True))
            raised = jnp.exp2((edge - top) * factor)
            total = jnp.sum(raised, axis=-1, keepdims=True)
            weights[h * tok : (h + 1) * tok, last - stretch : last] = raised.astype(bf)
            if b:
                raised = jnp.exp2((inner - top) * factor)
                total = total + jnp.sum(raised, axis=-1, keepdims=True)
                weights[h * tok : (h + 1) * tok, : last - stretch] = raised.astype(bf)
            sums.append(total)
        mixed = dot32(weights[:, :last], values[:last])
        total = None
        for h in range(heads):
            own = mixed[h * tok : (h + 1) * tok] / sums[h]
            total = own if total is None else jnp.where(lane < h, total, own)
        heads_out[b] = total.astype(bf)

        @pl.when(z != b)
        def _():
            remote(
                heads_out.at[b], token_in.at[z], so.at[b], ro.at[z], b * n_y + y
            ).start()

    token_in[z] = heads_out[z]
    for load in loads[small:]:
        load.wait()
    for k in range(1, n_z):
        other = (z + k) % n_z
        remote(
            heads_out.at[other], token_in.at[other], so.at[other], ro.at[other], other * n_y + y
        ).wait()
    square = None
    for s in range(n_z):
        piece = token_in[s].astype(f32)
        part = jnp.sum(piece * piece, axis=-1, keepdims=True)
        square = part if square is None else square + part
    scale = lax.rsqrt(square / (n_z * wide_v) + eps)
    mixed = jnp.concatenate(
        [
            (token_in[s].astype(f32) * scale * mix_gain_ref[:, s * wide_v : (s + 1) * wide_v]).astype(bf)
            for s in range(n_z)
        ],
        axis=1,
    )
    stream = residual_ref[...].astype(f32) + dot32(mixed, out_weight_ref[...])
    acc[...] = stream
    scale = lax.rsqrt(jnp.mean(stream * stream, axis=-1, keepdims=True) + eps)
    normed_ref[...] = (stream * scale * ffn_gain_ref[...]).astype(bf)

    first = {}

    def pack(k, target):
        picks = pick_ref[(z + k) % n_z]
        target[k, :, :width] = dot32(picks, normed_ref[...]).astype(bf)
        target[k, :, width:] = lax.dot_general(
            picks, info_ref[...], (((1,), (1,)), ((), ())), preferred_element_type=f32
        ).astype(bf)

    for k in (1, 3, 2):
        pack(k, out1)
        first[k] = remote(out1.at[k], in1.at[k], s1.at[k], r1.at[k], at_z(k))
        first[k].start()
    pack(0, in1)

    def slots(k):
        info = in1[k, :, width:].astype(f32)
        place = lax.broadcasted_iota(jnp.int32, (rows, peers * cap), 1).astype(f32)
        return place == info[:, 0:1], place == info[:, 1:2], info

    second = {}

    def scatter(k):
        if k:
            first[k].wait_recv()
        at0, at1, _ = slots(k)
        choose = (at0.astype(f32) + at1.astype(f32)).astype(bf)
        placed = dot_t(choose, in1[k, :, :width]).astype(bf)
        for e in range(peers):
            out2[k, e] = placed[e * cap : (e + 1) * cap]
        second[k] = [
            remote(
                out2.at[k, (mine + j) % peers], arrive.at[k, j], s2.at[k, j], r2.at[k, j], peer(j)
            )
            for j in range(1, peers)
        ]
        for copy in second[k]:
            copy.start()
        arrive[k, 0] = out2[k, mine]

    third = {}

    def serve(k):
        for copy in second[k]:
            copy.wait_recv()
        given = arrive[k].reshape(peers * cap, width)
        gate_act = dot32(given, gate_ref[...])
        upward = dot32(given, up_ref[...])
        hidden = (gate_act * (1.0 / (1.0 + jnp.exp(-gate_act))) * upward).astype(bf)
        result = dot32(hidden, down_ref[...]).astype(bf)
        for j in range(peers):
            served[k, j] = result[j * cap : (j + 1) * cap]
        third[k] = [
            remote(
                served.at[k, j], back2.at[k, mine], s3.at[k, j], r3.at[k, peers - j], peer(peers - j)
            )
            for j in range(1, peers)
        ]
        for copy in third[k]:
            copy.start()
        back2[k, mine] = served[k, 0]

    fourth = {}

    def merge(k):
        for copy in third[k]:
            copy.wait_recv()
        at0, at1, info = slots(k)
        high = jnp.where(at0, info[:, 2:3], 0.0) + jnp.where(at1, info[:, 4:5], 0.0)
        low = jnp.where(at0, info[:, 3:4], 0.0) + jnp.where(at1, info[:, 5:6], 0.0)
        got = back2[k].reshape(peers * cap, width)
        total = dot32(high.astype(bf), got) + dot32(low.astype(bf), got)
        if k:
            merged[k] = total.astype(bf)
            fourth[k] = remote(merged.at[k], home.at[k], s4.at[k], r4.at[k], at_z(n_z - k))
            fourth[k].start()
        else:
            acc[...] += dot_t(pick_ref[z], total.astype(bf))

    for k in (0, 1, 3, 2):
        scatter(k)
    for k in (1, 3, 2, 0):
        serve(k)
    for k in (1, 3, 2, 0):
        merge(k)
    for k in (1, 3, 2):
        fourth[k].wait_recv()
        acc[...] += dot_t(pick_ref[(z + k) % n_z], home[k])
    out_ref[...] = acc[...].astype(bf)
    for copy in list(down.values()) + sent + asked:
        copy.wait_send()
    for k in range(n_z):
        if k:
            first[k].wait_send()
            fourth[k].wait_send()
        for copy in second[k] + third[k]:
            copy.wait_send()


def trig(positions, nope, rope):
    frequency = 10000.0 ** (-2.0 * np.arange(rope // 2) / rope)
    angle = np.asarray(positions, np.float64)[:, None] * frequency[None, :]
    cos = np.ones((len(positions), 128))
    sin = np.zeros((len(positions), 128))
    cos[:, nope : nope + rope] = np.concatenate([np.cos(angle)] * 2, axis=1)
    sin[:, nope : nope + rope] = np.concatenate([np.sin(angle)] * 2, axis=1)
    return np.stack([cos, sin]).astype(np.float32)


def per_device(
    residual,
    query,
    latent,
    rope_key,
    latent_gain,
    query_gain,
    key_gain,
    key_weight,
    value_weight,
    mix_gain,
    out_weight,
    ffn_gain,
    expert_choice,
    group_prob,
    expert_prob,
    gate_weight,
    up_weight,
    down_weight,
):
    n_sp = lax.axis_size("sp")
    n_dp = lax.axis_size("dp")
    n_z = GROUPS
    n_y = n_sp // n_z
    tok, width = residual.shape[1:]
    rope = rope_key.shape[2]
    qk = query_gain.shape[0]
    nope = qk - rope
    lat = latent.shape[2]
    head_count = query.shape[2] // qk
    value_width = value_weight.shape[1] // head_count
    heads = head_count // n_z
    length = n_sp * tok
    half = rope // 2
    top = expert_choice.shape[2]
    peers = n_y * n_dp
    cap = tok // peers
    rows = tok // top
    hidden = gate_weight.shape[2]
    slot = 128
    wide_v = heads * value_width
    bf = jnp.bfloat16
    f32 = jnp.float32
    near = jnp.asarray(trig(np.arange(tok), nope, rope))
    far = jnp.asarray(trig(np.arange(n_sp) * tok, nope, rope))
    vmem = pltpu.VMEM
    hbm = pl.BlockSpec(memory_space=pl.ANY)
    dma = pltpu.SemaphoreType.DMA
    out = pl.pallas_call(
        functools.partial(
            layer_kernel, n_sp, n_y, n_dp, nope, rope, value_width, cap, top
        ),
        out_shape=jax.ShapeDtypeStruct((tok, width), bf),
        in_specs=[hbm] * 20,
        out_specs=pl.BlockSpec(memory_space=vmem),
        scratch_shapes=[
            vmem((tok, width), bf),
            vmem((tok, lat), bf),
            vmem((rope, tok), bf),
            vmem((1, lat), f32),
            vmem((1, qk), f32),
            vmem((1, qk), f32),
            vmem((lat, wide_v), bf),
            vmem((lat, wide_v), bf),
            vmem((1, head_count * value_width), f32),
            vmem(out_weight.shape, bf),
            vmem((1, width), f32),
            vmem((top, tok), jnp.int32),
            vmem((1, tok), f32),
            vmem((top, tok), f32),
            vmem((width, hidden), bf),
            vmem((width, hidden), bf),
            vmem((hidden, width), bf),
            vmem(near.shape, f32),
            vmem(far.shape, f32),
            vmem((lat, heads * slot), bf),
            vmem((heads * qk, heads * slot), bf),
            vmem((heads * qk, heads * slot), bf),
            vmem((n_z, tok, heads * qk), bf),
            vmem((tok + half, lat), bf),
            vmem((n_sp, tok + half, lat), bf),
            vmem((n_z, heads, tok, slot), bf),
            vmem((heads, length, slot), bf),
            vmem((length, wide_v), bf),
            vmem((tok, n_y * tok), f32),
            vmem((heads * tok, length), bf),
            vmem((n_z, tok, wide_v), bf),
            vmem((n_z, tok, wide_v), bf),
            vmem((tok, width), bf),
            vmem((slot, tok), bf),
            vmem((n_z, rows, tok), bf),
            vmem((n_z, rows, width + slot), bf),
            vmem((n_z, rows, width + slot), bf),
            vmem((n_z, peers, cap, width), bf),
            vmem((n_z, peers, cap, width), bf),
            vmem((n_z, peers, cap, width), bf),
            vmem((n_z, peers, cap, width), bf),
            vmem((n_z, rows, width), bf),
            vmem((n_z, rows, width), bf),
            vmem((tok, width), f32),
            dma((20,)),
            dma((n_z,)),
            dma((n_z,)),
            dma((n_z,)),
            dma((n_z,)),
            dma((n_z, n_y)),
            dma((n_z, n_y)),
            dma((n_z,)),
            dma((n_z,)),
            dma((n_z,)),
            dma((n_z,)),
            dma((n_z, peers)),
            dma((n_z, peers)),
            dma((n_z, peers)),
            dma((n_z, peers)),
            dma((n_z,)),
            dma((n_z,)),
        ],
        compiler_params=pltpu.CompilerParams(
            collective_id=0, has_side_effects=True, vmem_limit_bytes=67043328
        ),
    )(
        residual[0],
        query[0],
        latent[0],
        rope_key[0].T,
        latent_gain[None],
        query_gain[None],
        key_gain[None],
        key_weight,
        value_weight,
        mix_gain[None],
        out_weight,
        ffn_gain[None],
        expert_choice[0].T,
        group_prob,
        expert_prob[0].T,
        gate_weight[0],
        up_weight[0],
        down_weight[0],
        near,
        far,
    )
    return out[None]


def solution(mesh):
    return jax.shard_map(
        per_device,
        mesh=mesh,
        in_specs=(
            P("dp", "sp", None),
            P("dp", "sp", None),
            P("dp", "sp", None),
            P("dp", "sp", None),
            P(),
            P(),
            P(),
            P(),
            P(),
            P(),
            P(),
            P(),
            P("dp", "sp", None),
            P("dp", "sp"),
            P("dp", "sp", None),
            P(("sp", "dp"), None, None),
            P(("sp", "dp"), None, None),
            P(("sp", "dp"), None, None),
        ),
        out_specs=P("dp", "sp", None),
        check_vma=False,
    )
```

time: 125 us -> 102 us (0.82)
  the two profiles are of different devices: /device:TPU:0 before, /device:TPU:14 now
where the time goes in v2:
time: 102 us; the launch traced here: 101 us
  Pallas kernels  99.4 us (97%)
  local copies, waits for them, and re-layouts  1.88 us (2%)
    pallas_call x1, Pallas kernels, per_device(): pl.pallas_call(functools.partial(layer_kernel, n_sp, n_y, n_dp, nope, rop...  99.4 us

profile of v2, /device:TPU:14, one launch (start us, length us, event | category | flops | bytes accessed | tf_op | source)
XLA Modules:
  0.0 101.3 jit_solution(2472170578273103636)
XLA Ops:
  0.0 99.4 %shard_map.190 = bf16[128,2048]{1,0:T(8,128)(2,1)} custom-call(bf16[128,2048]{1,0:T(8,128)(2,1)} %bitcast.25, bf16[128,1536]{1,0:T(8,128)(2,1)} %bitcast.26, bf16[128,256]{1,0:T(8,128)(2,1)} %bitcast.27, bf16[32,128]{1,0:T(8,128)(2,1)} %bitcast.28, f32[1,256]{1,0:T(1,128)} %bitcast.31, f32[1,96]{1,0:T(1,128)} %bitcast.34, f32[1,96]{1,0:T(1,128)} %bitcast.35, ...), custom_call_target="tpu_custom_call" | custom-call | tf_op jit(solution)/shard_map/pallas_call | solution.py:611
  99.5 1.9 %copy.22 = bf16[1,128,2048]{2,1,0:T(8,128)(2,1)} copy(bf16[1,128,2048]{2,1,0:T(8,128)(2,1)} %bitcast.21) | data formatting | bytes 1048576

commit v3 on v2

--- a/solution.py
+++ b/solution.py
@@ -52,6 +52,9 @@
     down_hbm,
     near_hbm,
     far_hbm,
+    pick_query_hbm,
+    spread_key_hbm,
+    pick_rope_hbm,
     out_ref,
     residual_ref,
     latent_ref,
@@ -74,7 +77,8 @@
     far_ref,
     wide_key,
     pick_query,
-    turn_query,
+    spread_key,
+    pick_rope,
     queries_in,
     packed,
     packed_in,
@@ -102,8 +106,12 @@
     rq,
     sz,
     rz,
+    sv,
+    rv,
     sy,
     ry,
+    sx,
+    rx,
     so,
     ro,
     s1,
@@ -141,6 +149,9 @@
         (key_weight_hbm.at[:, own_part], key_weight_ref),
         (value_weight_hbm.at[:, own_part], value_weight_ref),
         (near_hbm, near_ref),
+        (pick_rope_hbm, pick_rope),
+        (spread_key_hbm, spread_key),
+        (pick_query_hbm, pick_query),
         (far_hbm, far_ref),
         (query_gain_hbm, query_gain_ref),
         (key_gain_hbm, key_gain_ref),
@@ -159,7 +170,7 @@
     loads = [
         pltpu.make_async_copy(src, dst, w_sem.at[n]) for n, (src, dst) in enumerate(pairs)
     ]
-    small = 15
+    small = 18
     for load in loads[:small]:
         load.start()
 
@@ -189,7 +200,9 @@
         return z * n_y + (y + m) % n_y
 
     barrier = pltpu.get_barrier_semaphore()
-    for target in [{"sp": at_z(k)} for k in range(1, n_z)] + [peer(j) for j in range(1, peers)]:
+    greeted = [{"sp": at_z(k)} for k in range(1, n_z)] + [{"sp": at_y(m)} for m in range(1, n_y)]
+    greeted += [{"dp": (dp + d) % n_dp} for d in range(1, n_dp)]
+    for target in greeted:
         pl.semaphore_signal(
             barrier, inc=1, device_id=target, device_id_type=pl.DeviceIdType.MESH
         )
@@ -200,43 +213,51 @@
     packed[:tok] = (raw * scale * latent_gain_ref[...]).astype(bf)
     packed[tok:, :tok] = rope_t_ref[:half]
     packed[tok:, tok:] = rope_t_ref[half:]
-    pl.semaphore_wait(barrier, n_z - 1 + peers - 1)
+    pl.semaphore_wait(barrier, len(greeted))
 
     sent = []
+    asked = []
     down = {}
+    over = {}
+    cut = packed.shape[0] * 5 // 9
+
+    def spread_y(k, source):
+        origin = at_z(n_z - k) if k else me
+        for m in (1, 3, 2):
+            copy = remote(
+                source, packed_in.at[origin, :cut], sy.at[k, m], ry.at[k, m], at_y(m)
+            )
+            copy.start()
+            sent.append(copy)
+
+    def spread_z(m, source):
+        origin = at_y(n_y - m) if m else me
+        for k in (1, 3, 2):
+            copy = remote(
+                source, packed_in.at[origin, cut:], sx.at[m, k], rx.at[m, k], at_z(k)
+            )
+            copy.start()
+            sent.append(copy)
+
+    def ask():
+        for k in (1, 3, 2):
+            target = (z + k) % n_z
+            copy = remote(query_part(target), queries_in.at[z], sq.at[k], rq.at[k], at_z(k))
+            copy.start()
+            asked.append(copy)
+
     for k in (1, 3, 2):
-        down[k] = remote(packed, packed_in.at[me], sz.at[k], rz.at[k], at_z(k))
+        down[k] = remote(
+            packed.at[:cut], packed_in.at[me, :cut], sz.at[k], rz.at[k], at_z(k)
+        )
         down[k].start()
-
-    def spread(k, source):
-        index = ((z + n_z - k) % n_z) * n_y + y
-        for m in (1, 3, 2):
-            sent.append(remote(source, packed_in.at[index], sy.at[k, m], ry.at[k, m], at_y(m)))
-            sent[-1].start()
-
-    spread(0, packed)
-    asked = []
-    for k in (1, 3, 2):
-        target = (z + k) % n_z
-        asked.append(remote(query_part(target), queries_in.at[z], sq.at[k], rq.at[k], at_z(k)))
-        asked[-1].start()
-
-    for load in loads[small:]:
-        load.start()
+        over[k] = remote(
+            packed.at[cut:], packed_in.at[me, cut:], sv.at[k], rv.at[k], at_y(k)
+        )
+        over[k].start()
+    spread_y(0, packed.at[:cut])
+    spread_z(0, packed.at[cut:])
     packed_in[me] = packed[...]
-
-    def selector(rows, columns, source):
-        i = lax.broadcasted_iota(jnp.int32, (rows, columns), 0)
-        c = lax.broadcasted_iota(jnp.int32, (rows, columns), 1)
-        return (i == source(c // slot, c % slot)).astype(f32).astype(bf)
-
-    def swapped(c):
-        return jnp.where(
-            c < nope, -1, jnp.where(c < nope + half, c + half, jnp.where(c < qk, c - half, -1))
-        )
-
-    def plain_of(c, first):
-        return jnp.where((c >= first) & (c < qk), c, -1)
 
     def route():
         lower = lax.broadcasted_iota(jnp.int32, (tok, tok), 0)
@@ -282,36 +303,23 @@
             total = jnp.where(at == n, jnp.broadcast_to(values_of, at.shape), total)
         info_ref[...] = total.astype(bf)
 
-    pick_query[...] = selector(
-        wide_q, heads * slot, lambda h, c: jnp.where(c < qk, c + h * qk, -1)
-    )
-    turn_query[...] = selector(
-        wide_q,
-        heads * slot,
-        lambda h, c: jnp.where((c >= nope) & (c < qk), swapped(c) + h * qk, -1),
-    )
-    pick_rope = selector(
-        rope,
-        2 * slot,
-        lambda h, c: jnp.where(
-            (c < nope) | (c >= qk), -1, jnp.where(h == 0, c, swapped(c)) - nope
-        ),
-    )
+    gaps = [(1, 1), (3, 3), (2, 2)]
+    for k, m in gaps:
+        down[k].wait_recv()
+        spread_y(k, packed_in.at[at_z(n_z - k), :cut])
+        over[m].wait_recv()
+        spread_z(m, packed_in.at[at_y(n_y - m), cut:])
+    ask()
+
+    for load in loads[small:]:
+        load.start()
+    for load in loads[3:small]:
+        load.wait()
     q_pos = y * tok + lax.broadcasted_iota(jnp.int32, bias.shape, 0)
     k_pos = lax.broadcasted_iota(jnp.int32, bias.shape, 1)
     bias[...] = jnp.where(k_pos // SPAN <= q_pos // SPAN, 0.0, -1e30)
-    loads[3].wait()
-    wide_key[...] = dot32(
-        key_weight_ref[...],
-        selector(heads * nope, heads * slot, lambda h, c: jnp.where(c < nope, c + h * nope, -1)),
-    ).astype(bf)
-    for load in loads[4:small]:
-        load.wait()
+    wide_key[...] = dot32(key_weight_ref[...], spread_key[...]).astype(bf)
     route()
-
-    for k in (1, 3, 2):
-        down[k].wait_recv()
-        spread(k, packed_in.at[((z + n_z - k) % n_z) * n_y + y])
 
     near_cos, near_sin = near_ref[0], near_ref[1]
 
@@ -346,7 +354,13 @@
 
         @pl.when(m > 0)
         def _():
-            remote(packed, packed_in.at[s], sy.at[k, m], ry.at[k, m], me).wait_recv()
+            part = packed_in.at[s, :cut]
+            remote(part, part, sy.at[k, m], ry.at[k, m], me).wait_recv()
+
+        @pl.when(k > 0)
+        def _():
+            part = packed_in.at[s, cut:]
+            remote(part, part, sx.at[m, k], rx.at[m, k], me).wait_recv()
 
         at = pl.ds(pl.multiple_of(s * tok, tok), tok)
         block = packed_in[s]
@@ -354,7 +368,7 @@
         values[at, :] = dot32(latent, value_weight_ref[...]).astype(bf)
         part = dot32(latent, wide_key[...]).astype(bf).astype(f32)
         turned_rows = jnp.concatenate([block[tok:, :tok], block[tok:, tok:]], axis=0)
-        spun = dot_t(turned_rows, pick_rope)
+        spun = dot_t(turned_rows, pick_rope[...])
         cos, sin = tables(s)
         plain_rope = spun[:, :slot]
         tail = plain_rope * (key_gain * cos) + spun[:, slot:] * (key_swap * sin)
@@ -372,8 +386,8 @@
 
     def prepare_queries(b, carry):
         raw = queries_in[b]
-        plain = dot32(raw, pick_query[...])
-        turned = dot32(raw, turn_query[...])
+        both_parts = dot32(raw, pick_query[...])
+        plain, turned = both_parts[:, : heads * slot], both_parts[:, heads * slot :]
         cos, sin = tables(b * n_y + y)
         for h in range(heads):
             span = slice(h * slot, (h + 1) * slot)
@@ -540,7 +554,7 @@
         fourth[k].wait_recv()
         acc[...] += dot_t(pick_ref[(z + k) % n_z], home[k])
     out_ref[...] = acc[...].astype(bf)
-    for copy in list(down.values()) + sent + asked:
+    for copy in list(down.values()) + list(over.values()) + sent + asked:
         copy.wait_send()
     for k in range(n_z):
         if k:
@@ -548,6 +562,41 @@
             fourth[k].wait_send()
         for copy in second[k] + third[k]:
             copy.wait_send()
+
+
+def selector(rows, columns, slot, source):
+    head, lane = np.divmod(np.arange(columns), slot)
+    origin = np.asarray([source(h, c) for h, c in zip(head, lane)])
+    return (np.arange(rows)[:, None] == origin[None, :]).astype(jnp.bfloat16)
+
+
+def selectors(heads, nope, rope, slot):
+    qk = nope + rope
+    half = rope // 2
+
+    def swapped(c):
+        return c + half if nope <= c < nope + half else c - half if nope + half <= c < qk else -1
+
+    def plain(h, c):
+        return c + h * qk if c < qk else -1
+
+    def turned(h, c):
+        return swapped(c) + h * qk if nope <= c < qk else -1
+
+    def shared(h, c):
+        return -1 if c < nope or c >= qk else (swapped(c) if h else c) - nope
+
+    query = np.concatenate(
+        [
+            selector(heads * qk, heads * slot, slot, plain),
+            selector(heads * qk, heads * slot, slot, turned),
+        ],
+        axis=1,
+    )
+    key = selector(
+        heads * nope, heads * slot, slot, lambda h, c: c + h * nope if c < nope else -1
+    )
+    return query, key, selector(rope, 2 * slot, slot, shared)
 
 
 def trig(positions, nope, rope):
@@ -605,6 +654,7 @@
     f32 = jnp.float32
     near = jnp.asarray(trig(np.arange(tok), nope, rope))
     far = jnp.asarray(trig(np.arange(n_sp) * tok, nope, rope))
+    picks, spreads, ropes = [jnp.asarray(m) for m in selectors(heads, nope, rope, slot)]
     vmem = pltpu.VMEM
     hbm = pl.BlockSpec(memory_space=pl.ANY)
     dma = pltpu.SemaphoreType.DMA
@@ -613,7 +663,7 @@
             layer_kernel, n_sp, n_y, n_dp, nope, rope, value_width, cap, top
         ),
         out_shape=jax.ShapeDtypeStruct((tok, width), bf),
-        in_specs=[hbm] * 20,
+        in_specs=[hbm] * 23,
         out_specs=pl.BlockSpec(memory_space=vmem),
         scratch_shapes=[
             vmem((tok, width), bf),
@@ -636,8 +686,9 @@
             vmem(near.shape, f32),
             vmem(far.shape, f32),
             vmem((lat, heads * slot), bf),
-            vmem((heads * qk, heads * slot), bf),
-            vmem((heads * qk, heads * slot), bf),
+            vmem(picks.shape, bf),
+            vmem(spreads.shape, bf),
+            vmem(ropes.shape, bf),
             vmem((n_z, tok, heads * qk), bf),
             vmem((tok + half, lat), bf),
             vmem((n_sp, tok + half, lat), bf),
@@ -660,13 +711,17 @@
             vmem((n_z, rows, width), bf),
             vmem((n_z, rows, width), bf),
             vmem((tok, width), f32),
-            dma((20,)),
-            dma((n_z,)),
-            dma((n_z,)),
-            dma((n_z,)),
-            dma((n_z,)),
+            dma((23,)),
+            dma((n_z,)),
+            dma((n_z,)),
+            dma((n_z,)),
+            dma((n_z,)),
+            dma((n_y,)),
+            dma((n_y,)),
             dma((n_z, n_y)),
             dma((n_z, n_y)),
+            dma((n_y, n_z)),
+            dma((n_y, n_z)),
             dma((n_z,)),
             dma((n_z,)),
             dma((n_z,)),
@@ -679,10 +734,10 @@
             dma((n_z,)),
         ],
         compiler_params=pltpu.CompilerParams(
-            collective_id=0, has_side_effects=True, vmem_limit_bytes=67043328
+            collective_id=0, has_side_effects=True, vmem_limit_bytes=50 * 1024 * 1024
         ),
     )(
-        residual[0],
+        *[pltpu.with_memory_space_constraint(v, pltpu.HBM) for v in (residual[0],
         query[0],
         latent[0],
         rope_key[0].T,
@@ -702,6 +757,9 @@
         down_weight[0],
         near,
         far,
+        picks,
+        spreads,
+        ropes)],
     )
     return out[None]
 

time: 102 us -> 96.7 us (0.948)
  the two profiles are of different devices: /device:TPU:14 before, /device:TPU:0 now
where the time goes in v3:
time: 96.7 us; the launch traced here: 96.6 us
  Pallas kernels  95.8 us (99%)
    pallas_call x1, Pallas kernels, per_device(): pl.pallas_call(functools.partial(layer_kernel, n_sp, n_y, n_dp, nope, rop...  95.8 us

profile of v3, /device:TPU:0, one launch (start us, length us, event | category | flops | bytes accessed | tf_op | source)
XLA Modules:
  0.0 96.6 jit_solution(13766119957161501564)
XLA Ops:
  0.0 95.8 %shard_map.217 = bf16[128,2048]{1,0:T(8,128)(2,1)S(1)} custom-call(bf16[128,2048]{1,0:T(8,128)(2,1)} %bitcast.25, bf16[128,1536]{1,0:T(8,128)(2,1)} %bitcast.26, bf16[128,256]{1,0:T(8,128)(2,1)} %bitcast.27, bf16[32,128]{1,0:T(8,128)(2,1)} %bitcast.28, f32[1,256]{1,0:T(1,128)} %bitcast.31, f32[1,96]{1,0:T(1,128)} %bitcast.34, f32[1,96]{1,0:T(1,128)} %bitcast.35, ...), custom_call_target="tpu_custom_call" | custom-call | tf_op jit(solution)/shard_map/pallas_call | solution.py:661
  95.8 0.8 copy.25

commit v4 on v3

--- a/solution.py
+++ b/solution.py
@@ -432,12 +432,14 @@
             own = mixed[h * tok : (h + 1) * tok] / sums[h]
             total = own if total is None else jnp.where(lane < h, total, own)
         heads_out[b] = total.astype(bf)
-
-        @pl.when(z != b)
-        def _():
-            remote(
-                heads_out.at[b], token_in.at[z], so.at[b], ro.at[z], b * n_y + y
-            ).start()
+        if b == 0:
+            for done in range(n_z - 1, -1, -1):
+
+                @pl.when(z != done)
+                def _():
+                    remote(
+                        heads_out.at[done], token_in.at[z], so.at[done], ro.at[z], done * n_y + y
+                    ).start()
 
     token_in[z] = heads_out[z]
     for load in loads[small:]:
@@ -474,11 +476,10 @@
             picks, info_ref[...], (((1,), (1,)), ((), ())), preferred_element_type=f32
         ).astype(bf)
 
-    for k in (1, 3, 2):
+    def launch(k):
         pack(k, out1)
         first[k] = remote(out1.at[k], in1.at[k], s1.at[k], r1.at[k], at_z(k))
         first[k].start()
-    pack(0, in1)
 
     def slots(k):
         info = in1[k, :, width:].astype(f32)
@@ -544,7 +545,12 @@
         else:
             acc[...] += dot_t(pick_ref[z], total.astype(bf))
 
-    for k in (0, 1, 3, 2):
+    pack(0, in1)
+    launch(1)
+    scatter(0)
+    launch(3)
+    launch(2)
+    for k in (1, 3, 2):
         scatter(k)
     for k in (1, 3, 2, 0):
         serve(k)

time: 96.7 us -> 92.4 us (0.956)
  Pallas kernels: 95.8 us -> 91.3 us
    pallas_call x1, Pallas kernels: 95.8 us -> 91.3 us  [per_device(): pl.pallas_call(functools.partial(layer_kernel, n_sp, n_y, n_dp, nope, rop...]
where the time goes in v4:
time: 92.4 us; the launch traced here: 92.1 us
  Pallas kernels  91.3 us (99%)
    pallas_call x1, Pallas kernels, per_device(): pl.pallas_call(functools.partial(layer_kernel, n_sp, n_y, n_dp, nope, rop...  91.3 us

profile of v4, /device:TPU:0, one launch (start us, length us, event | category | flops | bytes accessed | tf_op | source)
XLA Modules:
  0.0 92.1 jit_solution(16903702473626619163)
XLA Ops:
  0.0 91.3 %shard_map.217 = bf16[128,2048]{1,0:T(8,128)(2,1)S(1)} custom-call(bf16[128,2048]{1,0:T(8,128)(2,1)} %bitcast.25, bf16[128,1536]{1,0:T(8,128)(2,1)} %bitcast.26, bf16[128,256]{1,0:T(8,128)(2,1)} %bitcast.27, bf16[32,128]{1,0:T(8,128)(2,1)} %bitcast.28, f32[1,256]{1,0:T(1,128)} %bitcast.31, f32[1,96]{1,0:T(1,128)} %bitcast.34, f32[1,96]{1,0:T(1,128)} %bitcast.35, ...), custom_call_target="tpu_custom_call" | custom-call | tf_op jit(solution)/shard_map/pallas_call | solution.py:667
  91.3 0.8 copy.25

commit v5 on v4

--- a/solution.py
+++ b/solution.py
@@ -255,8 +255,8 @@
             packed.at[cut:], packed_in.at[me, cut:], sv.at[k], rv.at[k], at_y(k)
         )
         over[k].start()
+    spread_z(0, packed.at[cut:])
     spread_y(0, packed.at[:cut])
-    spread_z(0, packed.at[cut:])
     packed_in[me] = packed[...]
 
     def route():
@@ -311,8 +311,6 @@
         spread_z(m, packed_in.at[at_y(n_y - m), cut:])
     ask()
 
-    for load in loads[small:]:
-        load.start()
     for load in loads[3:small]:
         load.wait()
     q_pos = y * tok + lax.broadcasted_iota(jnp.int32, bias.shape, 0)
@@ -380,6 +378,8 @@
         return carry
 
     lax.fori_loop(0, n_sp, prepare, 0)
+    for load in loads[small:]:
+        load.start()
 
     for copy in asked:
         copy.wait_recv()
@@ -552,22 +552,24 @@
     launch(2)
     for k in (1, 3, 2):
         scatter(k)
-    for k in (1, 3, 2, 0):
+    def settle(copies):
+        for copy in copies:
+            copy.wait_send()
+
+    for k in (1, 3, 2):
         serve(k)
-    for k in (1, 3, 2, 0):
+    settle(list(down.values()) + list(over.values()) + sent + asked + list(first.values()))
+    serve(0)
+    settle(second[0] + second[1] + second[3] + second[2])
+    for k in (1, 3, 2):
         merge(k)
+    settle(third[1] + third[3])
+    merge(0)
     for k in (1, 3, 2):
         fourth[k].wait_recv()
         acc[...] += dot_t(pick_ref[(z + k) % n_z], home[k])
     out_ref[...] = acc[...].astype(bf)
-    for copy in list(down.values()) + list(over.values()) + sent + asked:
-        copy.wait_send()
-    for k in range(n_z):
-        if k:
-            first[k].wait_send()
-            fourth[k].wait_send()
-        for copy in second[k] + third[k]:
-            copy.wait_send()
+    settle(third[2] + third[0] + list(fourth.values()))
 
 
 def selector(rows, columns, slot, source):

time: 92.4 us -> 91.9 us (level)
  no operation moved by 1% of the time
where the time goes in v5:
time: 91.9 us; the launch traced here: 91.8 us
  Pallas kernels  91 us (99%)
    pallas_call x1, Pallas kernels, per_device(): pl.pallas_call(functools.partial(layer_kernel, n_sp, n_y, n_dp, nope, rop...  91 us

profile of v5, /device:TPU:0, one launch (start us, length us, event | category | flops | bytes accessed | tf_op | source)
XLA Modules:
  0.0 91.8 jit_solution(2264432955927829848)
XLA Ops:
  0.0 91.0 %shard_map.217 = bf16[128,2048]{1,0:T(8,128)(2,1)S(1)} custom-call(bf16[128,2048]{1,0:T(8,128)(2,1)} %bitcast.25, bf16[128,1536]{1,0:T(8,128)(2,1)} %bitcast.26, bf16[128,256]{1,0:T(8,128)(2,1)} %bitcast.27, bf16[32,128]{1,0:T(8,128)(2,1)} %bitcast.28, f32[1,256]{1,0:T(1,128)} %bitcast.31, f32[1,96]{1,0:T(1,128)} %bitcast.34, f32[1,96]{1,0:T(1,128)} %bitcast.35, ...), custom_call_target="tpu_custom_call" | custom-call | tf_op jit(solution)/shard_map/pallas_call | solution.py:669
  91.0 0.8 copy.25
